TPU v7x, 256 devices: a whole 4x4x8 slice. The times are simulated.
256 devices in a mesh: ep: 64 (over z, y, core), tp: 4 (over x).
Axes of the slice: x: 4, y: 4, z: 8, core: 2. Of those that a mesh axis runs over, the one named last changes fastest.
Arguments:
- queries: bfloat16 [65536, 512], P('ep', 'tp'), may hold values from -6 to 6
- keys: bfloat16 [65536, 512], P('ep', 'tp'), may hold values from -6 to 6
- values: bfloat16 [65536, 1024], P('ep', 'tp'), may hold values from -6 to 6
- decay_rate: float32 [8], P('tp'), may hold values from 4.577637e-06 to 0.0333333333, as said below
- ret_gain: float32 [1024], P('tp'), may hold values from 0.1 to 1.9
- w_out: bfloat16 [1024, 2048], P('tp'), may hold values from -0.1875 to 0.1875
- moe_in: bfloat16 [32768, 2048], P(('ep', 'tp')), may hold values from -6 to 6
- ffn_gain: float32 [2048], replicated, may hold values from 0.1 to 1.9
- routes: int32 [32768, 2], P(('ep', 'tp')), may hold values from 0 to 63, all different within a row; in each aligned block of 128 rows (0 to 127, 128 to 255, ...) at most 5 rows name the same one
- route_weight: float32 [32768, 2], P(('ep', 'tp')), may hold values from 0.2 to 1
- expert_gate: bfloat16 [64, 2048, 3072], P('ep', None, 'tp'), may hold values from -0.125 to 0.125
- expert_up: bfloat16 [64, 2048, 3072], P('ep', None, 'tp'), may hold values from -0.125 to 0.125
- expert_down: bfloat16 [64, 3072, 2048], P('ep', 'tp'), may hold values from -0.109375 to 0.109375
Outputs:
- mix_out: bfloat16 [65536, 2048], P(('ep', 'tp'))
- moe_out: bfloat16 [32768, 2048], P(('ep', 'tp'))
Inputs may be any that keep to these rules, and one draw needn't show every extreme that they name: `routes`: each row names 2 different experts. Among the 128 rows of one device no expert is named more than 5 times, and in every draw some device names some expert exactly 5 times. `decay_rate`: positive rates.
All inputs are finite; a program needn't handle non-finite values.
Results may differ from a plain program's by a relative error of at most 0.017.
Values may be sent and summed in bfloat16 or wider, within the bound.
No kernel may reach another device: no remote copies, remote signals or barrier semaphores. Data moves between devices by JAX's collectives and lax.ppermute only.
A program may use at most 128 MiB of HBM per device.

v0:
```python
import jax
import jax.numpy as jnp
from jax import lax
from jax.experimental import pallas as pl
from jax.experimental.pallas import tpu as pltpu
from jax.sharding import Mesh
from jax.sharding import PartitionSpec as P


DK = 64
DV = 128
LANES = 128
QBLOCK = 256
TILE = 256
LOOPS = 3
EP = ("ep_0", "ep_1", "ep_2")
EP_TP = ("ep_0", "ep_1", "ep_2", "tp")
SLOTS = ((0, 2), (2, 3))

EPS = 1e-06
ROPE_BASE = 10000.0
F32 = jnp.float32
BF16 = jnp.bfloat16


def params(mib=14):
    return pltpu.CompilerParams(vmem_limit_bytes=mib * 1024 * 1024)


def cost(flops, num_bytes):
    return pl.CostEstimate(flops=int(flops), bytes_accessed=int(num_bytes), transcendentals=0)


def split(x):
    high = x.astype(BF16)
    return high, (x - high.astype(F32)).astype(BF16)


def product(a, b, dims):
    def dot(x, y):
        return lax.dot_general(x, y, (dims, ((), ())), preferred_element_type=F32)

    a_high, a_low = split(a)
    if b.dtype == BF16:
        return dot(a_high, b) + dot(a_low, b)
    b_high, b_low = split(b)
    return dot(a_high, b_high) + (dot(a_high, b_low) + dot(a_low, b_high))


PLAIN = ((1,), (0,))
RIGHT = ((1,), (1,))
LEFT = ((0,), (0,))


def place(x, gain, routes, experts, cap):
    rows, width = x.shape
    cuts = width // LANES
    lines = experts * cap

    def body(x_ref, g_ref, r_ref, o_ref, slot_ref, scr, flat):
        xf = x_ref[...].astype(F32)
        normed = (
            xf * lax.rsqrt(jnp.mean(xf * xf, axis=-1, keepdims=True) + EPS) * g_ref[...]
        ).astype(BF16)
        r0 = r_ref[:, 0:1]
        r1 = r_ref[:, 1:2]
        ids = lax.broadcasted_iota(jnp.int32, (rows, experts), 1)
        h0 = r0 == ids
        h1 = r1 == ids
        hits = jnp.where(h0 | h1, 1.0, 0.0).astype(BF16)
        tri = jnp.where(
            lax.broadcasted_iota(jnp.int32, (rows, rows), 0)
            > lax.broadcasted_iota(jnp.int32, (rows, rows), 1),
            1.0,
            0.0,
        ).astype(BF16)
        before = jnp.dot(tri, hits, preferred_element_type=F32)
        s0 = jnp.sum(jnp.where(h0, before, 0.0), axis=1, keepdims=True).astype(jnp.int32)
        s1 = jnp.sum(jnp.where(h1, before, 0.0), axis=1, keepdims=True).astype(jnp.int32)
        slot_ref[:, 0:1] = s0
        slot_ref[:, 1:2] = s1
        col = lax.broadcasted_iota(jnp.int32, (rows, lines), 1)
        hot = (col == r0 * cap + s0) | (col == r1 * cap + s1)
        hot = jnp.where(hot, 1.0, 0.0).T.astype(BF16)
        flat[...] = jnp.dot(hot, normed, preferred_element_type=F32)

        @pl.loop(0, cuts // 4)
        def _(n):
            for i in range(4):
                c = 4 * n + i
                cols = pl.ds(pl.multiple_of(c * LANES, LANES), LANES)
                scr[pl.ds(c, lines, stride=cuts), :] = flat[:, cols]

        o_ref[...] = scr[...].astype(BF16)

    return pl.pallas_call(
        body,
        out_shape=[
            jax.ShapeDtypeStruct((lines * cuts, LANES), BF16),
            jax.ShapeDtypeStruct((rows, 2), jnp.int32),
        ],
        scratch_shapes=[pltpu.VMEM((lines * cuts, LANES), F32), pltpu.VMEM((lines, width), F32)],
        compiler_params=params(20),
        cost_estimate=cost(2 * rows * lines * width, 4 * x.size),
    )(x, gain.reshape(1, width), routes)


def unpack(lines, width, groups, cap):
    cuts = width // LANES
    half = groups // 2

    def body(x_ref, *refs):
        outs, scr = refs[:-1], refs[-1]
        scr[...] = x_ref[...].astype(F32)

        @pl.loop(0, cuts)
        def _(c):
            cols = pl.ds(pl.multiple_of(c * LANES, LANES), LANES)
            for n, (first, count) in enumerate(SLOTS):
                for side in range(2):
                    for s in range(count):
                        start = side * half * cap * cuts + (first + s) * cuts + c
                        row = (n * side * count + s) * half
                        outs[2 if n else side][row : row + half, cols] = scr[
                            pl.ds(start, half, stride=cap * cuts), :
                        ].astype(BF16)

    near, late = (count * half for _, count in SLOTS)
    return pl.pallas_call(
        body,
        out_shape=[jax.ShapeDtypeStruct((size, width), BF16) for size in (near, near, 2 * late)],
        scratch_shapes=[pltpu.VMEM(lines.shape, F32)],
        compiler_params=params(16),
        cost_estimate=cost(2e9, 4 * lines.size),
    )(lines)


def add_pack(terms, count):
    rows, width = terms[0][0].shape
    part = rows // 2
    cuts = width // LANES
    half = part // count
    sizes = [len(term) for term in terms]

    def body(*refs):
        o_ref, scr = refs[-2:]

        @pl.loop(0, cuts)
        def _(c):
            cols = pl.ds(pl.multiple_of(c * LANES, LANES), LANES)
            for side in range(2):
                for s in range(count):
                    total = 0.0
                    at = 0
                    for size in sizes:
                        row = s * half + (side * part if size == 1 else 0)
                        ref = refs[at + (side if size == 2 else 0)]
                        total = total + ref[row : row + half, cols].astype(F32)
                        at += size
                    start = side * half * count * cuts + s * cuts + c
                    scr[pl.ds(start, half, stride=count * cuts), :] = total

        o_ref[...] = scr[...].astype(BF16)

    return pl.pallas_call(
        body,
        out_shape=jax.ShapeDtypeStruct((rows * cuts, LANES), BF16),
        scratch_shapes=[pltpu.VMEM((rows * cuts, LANES), F32)],
        compiler_params=params(),
        cost_estimate=cost(2e9, 8 * rows * width),
    )(*[x for term in terms for x in term])


def expert(blocks, w_gate, w_up, w_down, loops, ranges):
    sizes = [block.shape[0] for block in blocks]
    width = blocks[0].shape[1]
    number = len(blocks)
    units = w_gate.shape[1]
    steps = units // TILE
    total = sum(sizes)
    rows = total // loops

    def body(*refs):
        ins, (g_ref, u_ref, d_ref) = refs[:number], refs[number : number + 3]
        outs, (x_scr, acc) = refs[number + 3 : -2], refs[-2:]
        step = pl.program_id(0)

        @pl.when(step == 0)
        def _():
            first = 0
            for size, ref in zip(sizes, ins):
                x_scr[first : first + size, :] = ref[...]
                first += size

        def block(at, first):
            x = x_scr[at, :]
            gate = jnp.dot(x, g_ref[...], preferred_element_type=F32)
            up = jnp.dot(x, u_ref[...], preferred_element_type=F32)
            hidden = (gate / (1.0 + jnp.exp(-gate)) * up).astype(BF16)
            out = jnp.dot(hidden, d_ref[...], preferred_element_type=F32)
            acc[at, :] = jnp.where(first, out, acc[at, :] + out)

        if loops == 1:
            block(slice(0, rows), step == 0)
        else:

            @pl.loop(0, loops)
            def _(i):
                block(pl.ds(pl.multiple_of(i * rows, rows), rows), step == 0)

        @pl.when(step == steps - 1)
        def _():
            for (low, high), ref in zip(ranges, outs):
                ref[...] = acc[low:high, :].astype(BF16)

    def whole(size):
        return pl.BlockSpec((size, width), lambda i: (0, 0))

    given = [high - low for low, high in ranges]
    return pl.pallas_call(
        body,
        grid=(steps,),
        in_specs=[whole(size) for size in sizes]
        + [
            pl.BlockSpec((width, TILE), lambda i: (0, i)),
            pl.BlockSpec((width, TILE), lambda i: (0, i)),
            pl.BlockSpec((TILE, width), lambda i: (i, 0)),
        ],
        out_specs=[whole(size) for size in given],
        out_shape=[jax.ShapeDtypeStruct((size, width), BF16) for size in given],
        scratch_shapes=[
            pltpu.VMEM((total, width), BF16),
            pltpu.VMEM((total, width), F32),
        ],
        compiler_params=params(36),
        cost_estimate=cost(6 * total * width * units, 6 * width * units),
    )(*blocks, w_gate, w_up, w_down)


def add(whole, term, first):
    rows = term.shape[0]

    def body(a_ref, b_ref, o_ref):
        if rows < whole.shape[0]:
            o_ref[...] = a_ref[...]
        at = slice(first, first + rows)
        o_ref[at, :] = (a_ref[at, :].astype(F32) + b_ref[...].astype(F32)).astype(BF16)

    return pl.pallas_call(
        body,
        out_shape=jax.ShapeDtypeStruct(whole.shape, BF16),
        compiler_params=params(6),
        cost_estimate=cost(1e9, 6 * whole.size),
    )(whole, term)


def mix(ys, ws):
    rows, deep = ys[0].shape
    width = ws[0].shape[1]
    tile = 512

    def body(*refs):
        y_refs, w_refs, o_ref = refs[:4], refs[4:9], refs[9]
        total = sum(
            jnp.dot(y[...], w[...], preferred_element_type=F32)
            for y, w in zip(y_refs[:3], w_refs[:3])
        )
        for n in range(2):
            cols = slice(n * deep // 2, (n + 1) * deep // 2)
            total += jnp.dot(y_refs[3][:, cols], w_refs[3 + n][...], preferred_element_type=F32)
        o_ref[...] = total.astype(BF16)

    return pl.pallas_call(
        body,
        grid=(width // tile,),
        in_specs=[pl.BlockSpec(y.shape, lambda i: (0, 0)) for y in ys]
        + [pl.BlockSpec((w.shape[0], tile), lambda i: (0, i)) for w in ws],
        out_specs=pl.BlockSpec((rows, tile), lambda i: (0, i)),
        out_shape=jax.ShapeDtypeStruct((rows, width), BF16),
        compiler_params=params(),
        cost_estimate=cost(3e9, 6e6),
    )(*ys, *ws)


def combine(chunks, routes, slots, weight, experts, width):
    rows = routes.shape[0]
    cuts = width // LANES

    def body(*refs):
        ins, (r_ref, s_ref, w_ref, o_ref, scr, acc) = refs[: len(SLOTS)], refs[len(SLOTS) :]
        w0 = w_ref[:, 0:1]
        w1 = w_ref[:, 1:2]
        for n, ((first, count), x_ref) in enumerate(zip(SLOTS, ins)):
            lines = experts * count
            scr[0 : lines * cuts, :] = x_ref[...].astype(F32)
            col = lax.broadcasted_iota(jnp.int32, (rows, lines), 1)
            hot = []
            for k in range(2):
                r = r_ref[:, k : k + 1]
                s = s_ref[:, k : k + 1]
                d = jnp.where((s >= first) & (s < first + count), r * count + s - first, -1)
                hot.append(jnp.where(col == d, 1.0, 0.0).astype(BF16))
            both = jnp.concatenate(hot, axis=0)

            wide = cuts // 4

            @pl.loop(0, cuts // wide)
            def _(c):
                cols = pl.ds(pl.multiple_of(c * wide * LANES, wide * LANES), wide * LANES)
                part = jnp.concatenate(
                    [
                        scr[pl.ds(wide * c + i, lines, stride=cuts), :].astype(BF16)
                        for i in range(wide)
                    ],
                    axis=1,
                )
                got = jnp.dot(both, part, preferred_element_type=F32)
                term = w0 * got[:rows] + w1 * got[rows:]
                if n == 0:
                    acc[:, cols] = term
                else:
                    acc[:, cols] += term

        o_ref[...] = acc[...].astype(BF16)

    most = max(count for _, count in SLOTS)
    return pl.pallas_call(
        body,
        out_shape=jax.ShapeDtypeStruct((rows, width), BF16),
        scratch_shapes=[
            pltpu.VMEM((experts * most * cuts, LANES), F32),
            pltpu.VMEM((rows, width), F32),
        ],
        compiler_params=params(),
        cost_estimate=cost(4 * rows * experts * 5 * width, 4 * rows * width),
    )(*chunks, routes, slots, weight)


def retain(queries, keys, values, coarse, fine, decay_rate):
    span, wide = queries.shape
    heads = wide // DK
    half = DK // 2
    steps = coarse[0].shape[0]
    step = span // steps

    def body(r_ref, q_ref, k_ref, v_ref, cc_ref, cs_ref, fc_ref, fs_ref, y_ref, qd_ref, st_ref, q_scr, k_scr):
        lane = lax.broadcasted_iota(jnp.int32, (step, wide), 1)
        first = lane % DK < half
        sign = jnp.where(first, -1.0, 1.0)

        @pl.loop(0, steps)
        def _(n):
            rows = pl.ds(pl.multiple_of(n * step, step), step)
            c_cos = cc_ref[pl.ds(n, 1), :]
            c_sin = cs_ref[pl.ds(n, 1), :]
            cos = c_cos * fc_ref[...] - c_sin * fs_ref[...]
            sin = (c_sin * fc_ref[...] + c_cos * fs_ref[...]) * sign

            def turned(x):
                other = jnp.where(first, pltpu.roll(x, wide - half, 1), pltpu.roll(x, half, 1))
                return x * cos + other * sin

            q_scr[rows, :] = turned(q_ref[rows, :].astype(F32)) * DK ** (-0.5)
            k_scr[rows, :] = turned(k_ref[rows, :].astype(F32))

        i = lax.broadcasted_iota(jnp.int32, (QBLOCK, QBLOCK), 0)
        j = lax.broadcasted_iota(jnp.int32, (QBLOCK, QBLOCK), 1)
        diff = (i - j).astype(F32)
        at = lax.broadcasted_iota(jnp.int32, (QBLOCK, DK), 0).astype(F32)
        for h in range(heads):
            rate = r_ref[h]
            dmat = jnp.where(diff >= 0, jnp.exp(-rate * jnp.maximum(diff, 0.0)), 0.0)
            q_fall = jnp.exp(-rate * (at + 1.0))
            k_fall = jnp.exp(-rate * (QBLOCK - 1.0 - at))
            block_fall = jnp.exp(jnp.full((DK, DV), -rate * QBLOCK, F32))

            def block(b, state):
                rows = pl.ds(pl.multiple_of(b * QBLOCK, QBLOCK), QBLOCK)
                q = q_scr[rows, h * DK : (h + 1) * DK]
                k = k_scr[rows, h * DK : (h + 1) * DK]
                v = v_ref[rows, h * DV : (h + 1) * DV]
                scores = product(q, k, RIGHT) * dmat
                y_ref[rows, h * DV : (h + 1) * DV] = product(scores, v, PLAIN) + product(
                    q * q_fall, state, PLAIN
                )
                past = (b * QBLOCK).astype(F32)
                qd_ref[rows, h * DK : (h + 1) * DK] = q * jnp.exp(-rate * (at + (past + 1.0)))
                return state * block_fall + product(k * k_fall, v, LEFT)

            state = lax.fori_loop(0, span // QBLOCK, block, jnp.zeros((DK, DV), F32))
            st_ref[h * DK : (h + 1) * DK, :] = state

    return pl.pallas_call(
        body,
        in_specs=[pl.BlockSpec(memory_space=pltpu.SMEM)] + [pl.BlockSpec()] * 7,
        out_shape=[
            jax.ShapeDtypeStruct((span, heads * DV), F32),
            jax.ShapeDtypeStruct((span, wide), F32),
            jax.ShapeDtypeStruct((wide, DV), F32),
        ],
        scratch_shapes=[pltpu.VMEM((span, wide), F32), pltpu.VMEM((span, wide), F32)],
        compiler_params=params(),
        cost_estimate=cost(8e9, 4 * span * wide * 8),
    )(decay_rate, queries, keys, values, *coarse, *fine)


def falls(r_ref, heads, steps):
    return jnp.concatenate(
        [jnp.exp(jnp.full((DK, DV), -1.0, F32) * (r_ref[h] * steps)) for h in range(heads)], axis=0
    )


SMEM = pl.BlockSpec(memory_space=pltpu.SMEM)


def chip_state(end, other, rate, at):
    heads = rate.shape[0]

    def body(r_ref, at_ref, e_ref, o_ref, t_ref):
        late = at_ref[2] == 1
        first = jnp.where(late, o_ref[...], e_ref[...])
        last = jnp.where(late, e_ref[...], o_ref[...])
        t_ref[...] = first * falls(r_ref, heads, 1.0) + last

    return pl.pallas_call(
        body,
        in_specs=[SMEM, SMEM] + [pl.BlockSpec()] * 2,
        out_shape=jax.ShapeDtypeStruct(end.shape, F32),
        compiler_params=params(4),
    )(rate, at, end, other)


def step_state(far, got, rate, spans):
    heads = rate.shape[0]

    def body(r_ref, f_ref, g_ref, o_ref):
        o_ref[...] = f_ref[...] + g_ref[...] * falls(r_ref, heads, float(spans))

    return pl.pallas_call(
        body,
        in_specs=[SMEM] + [pl.BlockSpec()] * 2,
        out_shape=jax.ShapeDtypeStruct(far.shape, F32),
        compiler_params=params(4),
    )(rate, far, got)


def finish(inner, q_fallen, other, far, got, gain, rate, at, spans, tensor):
    span, wide = inner.shape
    heads = wide // DV
    share = span // tensor

    def body(r_ref, at_ref, y_ref, q_ref, o_ref, f_ref, l_ref, g_ref, *refs):
        outs, st = refs[:-1], refs[-1]
        c = at_ref[2]
        me = at_ref[3]
        past = f_ref[...] + l_ref[...] * falls(r_ref, heads, float(spans))
        st[...] = jnp.where(c == 1, o_ref[...], 0.0) + past * falls(r_ref, heads, c.astype(F32))
        for away, out in zip((0, 1, 3, 2), outs):
            block = lax.rem(me + away, tensor)
            rows = pl.ds(pl.multiple_of(block * share, share), share)
            for h in range(heads):
                cols = slice(h * DV, (h + 1) * DV)
                ret = y_ref[rows, cols] + product(
                    q_ref[rows, h * DK : (h + 1) * DK], st[h * DK : (h + 1) * DK, :], PLAIN
                )
                mean_sq = jnp.mean(ret * ret, axis=-1, keepdims=True)
                out[:, cols] = (ret * lax.rsqrt(mean_sq + EPS) * g_ref[:, cols]).astype(BF16)

    return pl.pallas_call(
        body,
        in_specs=[SMEM, SMEM] + [pl.BlockSpec()] * 6,
        out_shape=[jax.ShapeDtypeStruct((share, wide), BF16)] * tensor,
        scratch_shapes=[pltpu.VMEM((heads * DK, DV), F32)],
        compiler_params=params(),
        cost_estimate=cost(2e9, 8 * span * wide),
    )(rate, at, inner, q_fallen, other, far, got, gain.reshape(1, wide))


def program(
    queries,
    keys,
    values,
    decay_rate,
    ret_gain,
    w_out,
    moe_in,
    ffn_gain,
    routes,
    route_weight,
    expert_gate,
    expert_up,
    expert_down,
):
    tensor = lax.axis_size("tp")
    groups = lax.axis_size(EP)
    span = queries.shape[0]
    heads = decay_rate.shape[0]
    rows, width = moe_in.shape
    experts = groups
    cap = 5 * rows * routes.shape[1] // (4 * experts)
    cuts = width // LANES
    to_right = [(i, (i + 1) % tensor) for i in range(tensor)]
    to_left = [(i, (i - 1) % tensor) for i in range(tensor)]
    across = [(i, (i + 2) % tensor) for i in range(tensor)]
    me = lax.axis_index("tp").astype(jnp.int32)
    w_half = w_out.shape[0] // 2

    def send(x, to):
        return lax.ppermute(x, "tp", to)

    w_left = send(w_out, to_right)
    w_right = send(w_out, to_left)

    sent, slots = place(moe_in, ffn_gain, routes, experts, cap)
    w_gate = expert_gate[0]
    w_up = expert_up[0]
    w_down = expert_down[0]

    n_z, n_y, n_c = (lax.axis_size(axis) for axis in EP)
    place_of = [lax.axis_index(axis) for axis in EP]
    at = jnp.stack([*place_of, me]).astype(jnp.int32)
    rate = decay_rate * span
    step = 32
    here = lax.axis_index(EP) * span
    half = DK // 2
    inv_freq = ROPE_BASE ** (-jnp.arange(half, dtype=F32) / half)
    coarse = (here + step * jnp.arange(span // step)).astype(F32)
    count = coarse.shape[0]
    angle = jnp.concatenate([coarse, jnp.arange(step, dtype=F32)])[:, None] * inv_freq[None, :]
    cosine = jnp.concatenate([jnp.cos(angle)] * (2 * heads), axis=1)
    sine = jnp.concatenate([jnp.sin(angle)] * (2 * heads), axis=1)
    coarse = (cosine[:count], sine[:count])
    fine = (cosine[count:], sine[count:])
    inner, q_fallen, end = retain(queries, keys, values, coarse, fine, decay_rate)

    arrived = lax.all_to_all(
        sent.reshape(experts, cap * cuts, LANES), EP, split_axis=0, concat_axis=0, tiled=True
    )
    owns = unpack(arrived.reshape(-1, LANES), width, groups, cap)

    answers = []
    for n, (_, count) in enumerate(SLOTS):
        last = n == len(SLOTS) - 1
        if last:
            own = owns[2]
            part = own.shape[0] // 2
            left = send(own, to_right)
            right = send(own, to_left)
            far_a = send(left[:part], to_right)
            far_b = send(right[part:], to_left)
            blocks = (own, left, right)
            ranges = [(0, 2), (2, 3), (3, 4), (4, 5), (5, 6)]
        else:
            own_a, own_b = owns[:2]
            part = own_a.shape[0]
            left_a = send(own_a, to_right)
            right_b = send(own_b, to_left)
            left_b = send(own_b, to_right)
            right_a = send(own_a, to_left)
            far_a = send(left_a, to_right)
            far_b = send(right_b, to_left)
            blocks = (own_a, own_b, left_a, left_b, right_a, right_b)
            ranges = [(0, 2), (2, 4), (4, 6)]
        ranges = [(low * part, high * part) for low, high in ranges]
        o_all, *parts = expert(blocks, w_gate, w_up, w_down, LOOPS, ranges)
        f_a, f_b = expert((far_a, far_b), w_gate, w_up, w_down, 1, [(0, part), (part, 2 * part)])
        via_a = send(f_a, to_right)
        via_b = send(f_b, to_left)
        if last:
            l_a, l_b, r_a, r_b = parts
            got_lb = [send(r_b, to_right)]
            got_ra = [send(l_a, to_left)]
        else:
            l_b, r_a = parts
            got_lb, got_ra = [], []
        r_sum = add(r_a, via_a, 0)
        l_sum = add(l_b, via_b, 0 if last else via_b.shape[0])
        got_l = [send(r_sum, to_right), *got_lb]
        got_r = [*got_ra, send(l_sum, to_left)]
        packed = add_pack(([o_all], got_l, got_r), count)
        answers.append(
            lax.all_to_all(
                packed.reshape(experts, count * cuts, LANES),
                EP,
                split_axis=0,
                concat_axis=0,
                tiled=True,
            ).reshape(-1, LANES)
        )

    other = lax.ppermute(end, EP[2], [(i, (i + 1) % n_c) for i in range(n_c)])
    total = chip_state(end, other, rate, at)
    chips = n_z * n_y

    def ahead(x, k):
        return lax.ppermute(x, EP[:2], [(i, i + k) for i in range(chips - k)])

    far = ahead(total, 1)
    k = 1
    while True:
        got = ahead(far, k)
        spans = n_c * k
        if 2 * k >= chips:
            break
        far = step_state(far, got, rate, spans)
        k *= 2
    y_own, y_r, y_l, y_f = finish(
        inner, q_fallen, other, far, got, ret_gain, rate, at, spans, tensor
    )
    y_left = send(y_r, to_right)
    y_right = send(y_l, to_left)
    y_far = send(y_f, across)
    w_halves = (w_left[:w_half], w_right[w_half:])
    w_far_a = send(w_halves[0], to_right)
    w_far_b = send(w_halves[1], to_left)
    mix_out = mix(
        (y_own, y_left, y_right, y_far), (w_out, w_left, w_right, w_far_a, w_far_b)
    )
    moe_out = combine(answers, routes, slots, route_weight, experts, width)
    return (mix_out, moe_out)


def solution(mesh):
    split = Mesh(mesh.devices.reshape(8, 4, 2, mesh.shape["tp"]), ("ep_0", "ep_1", "ep_2", "tp"))
    in_specs = (
        P(EP, "tp"),
        P(EP, "tp"),
        P(EP, "tp"),
        P("tp"),
        P("tp"),
        P("tp", None),
        P(EP_TP, None),
        P(),
        P(EP_TP, None),
        P(EP_TP, None),
        P(EP, None, "tp"),
        P(EP, None, "tp"),
        P(EP, "tp", None),
    )
    out_specs = (P(EP_TP, None), P(EP_TP, None))
    return jax.shard_map(program, mesh=split, in_specs=in_specs, out_specs=out_specs, check_vma=False)
```

profile of v0, /device:TPU:8, one launch (start us, length us, event | category | flops | bytes accessed | tf_op | source)
XLA Modules:
  0.0 292.1 jit_solution(1920856501877415182)
XLA Ops:
  3.2 2.6 shard_map.148
  5.7 46.3 %all_to_all.15 = bf16[64,80,128]{2,1,0:T(8,128)(2,1)S(1)} all-to-all(bf16[64,80,128]{2,1,0:T(8,128)(2,1)S(1)} %bitcast.29), channel_id=1, replica_groups=mesh['ep_0'=8,'ep_1'=4,'ep_2'=2,'tp'=4] {'ep_0','ep_1','ep_2'}, dimensions={0} | all-to-all | bytes 2621440 | tf_op jit(solution)/shard_map/all_to_all | solution.py:536
  52.0 2.7 shard_map.149
  57.9 4.9 %collective-permute-done.14.refs_2_ = bf16[64,2048]{1,0:T(8,128)(2,1)S(1)} collective-permute-done((bf16[64,2048]{1,0:T(8,128)(2,1)}, bf16[64,2048]{1,0:T(8,128)(2,1)S(1)}, u32[]{:S(2)}, u32[]{:S(2)}) %collective-permute-start.14) | collective-permute-done | bytes 262176 | tf_op jit(solution)/shard_map/ppermute | solution.py:509
  65.3 1.8 collective-permute-start.25
  69.1 4.1 %collective-permute-done.18.refs_0_ = bf16[64,2048]{1,0:T(8,128)(2,1)S(1)} collective-permute-done((bf16[64,2048]{1,0:T(8,128)(2,1)S(1)}, bf16[64,2048]{1,0:T(8,128)(2,1)S(1)}, u32[]{:S(2)}, u32[]{:S(2)}) %collective-permute-start.18) | collective-permute-done | bytes 262176 | tf_op jit(solution)/shard_map/ppermute | solution.py:509
  73.5 17.0 %collective-permute-done.19.refs_1_ = bf16[64,2048]{1,0:T(8,128)(2,1)} collective-permute-done((bf16[64,2048]{1,0:T(8,128)(2,1)}, bf16[64,2048]{1,0:T(8,128)(2,1)}, u32[]{:S(2)}, u32[]{:S(2)}) %collective-permute-start.19) | collective-permute-done | bytes 262176 | tf_op jit(solution)/shard_map/ppermute | solution.py:509
  91.8 1.9 copy-done.1
  93.6 1.9 copy-done.4
  95.5 3.7 %shard_map.151 = (bf16[64,2048]{1,0:T(8,128)(2,1)S(1)}, bf16[64,2048]{1,0:T(8,128)(2,1)S(1)}) custom-call(bf16[64,2048]{1,0:T(8,128)(2,1)S(1)} %collective-permute-done.18.refs_0_, bf16[64,2048]{1,0:T(8,128)(2,1)} %collective-permute-done.19.refs_1_, bf16[2048,768]{1,0:T(8,128)(2,1)S(1)} %bitcast.15, bf16[2048,768]{1,0:T(8,128)(2,1)S(1)} %bitcast.19, ...), custom_call_target="tpu_custom_call" | custom-call | flops 1207959552 | bytes 9437184 | tf_op jit(solution)/shard_map/pallas_call | solution.py:220
  99.2 2.1 collective-permute-start.22
  101.3 8.4 %shard_map.150 = (bf16[128,2048]{1,0:T(8,128)(2,1)S(1)}, bf16[128,2048]{1,0:T(8,128)(2,1)S(1)}, bf16[128,2048]{1,0:T(8,128)(2,1)S(1)}) custom-call(bf16[64,2048]{1,0:T(8,128)(2,1)} %get-tuple-element.34.refs_0_, bf16[64,2048]{1,0:T(8,128)(2,1)} %get-tuple-element.35.refs_1_, bf16[64,2048]{1,0:T(8,128)(2,1)S(1)} %copy-done.13, ...), custom_call_target="tpu_custom_call" | custom-call | flops 3623878656 | bytes 9437184 | tf_op jit(solution)/shard_map/pallas_call | solution.py:220
  115.3 2.1 collective-permute-start.23
  117.3 6.4 %collective-permute-done.20.b_ref = bf16[64,2048]{1,0:T(8,128)(2,1)S(1)} collective-permute-done((bf16[64,2048]{1,0:T(8,128)(2,1)S(1)}, bf16[64,2048]{1,0:T(8,128)(2,1)S(1)}, u32[]{:S(2)}, u32[]{:S(2)}) %collective-permute-start.20) | collective-permute-done | bytes 262176 | tf_op jit(solution)/shard_map/ppermute | solution.py:509
  124.4 7.8 %collective-permute-done.26.refs_0_ = bf16[96,2048]{1,0:T(8,128)(2,1)S(1)} collective-permute-done((bf16[96,2048]{1,0:T(8,128)(2,1)S(1)}, bf16[96,2048]{1,0:T(8,128)(2,1)S(1)}, u32[]{:S(2)}, u32[]{:S(2)}) %collective-permute-start.26) | collective-permute-done | bytes 393248 | tf_op jit(solution)/shard_map/ppermute | solution.py:509
  132.2 4.2 %shard_map.156 = (bf16[96,2048]{1,0:T(8,128)(2,1)}, bf16[96,2048]{1,0:T(8,128)(2,1)}) custom-call(bf16[96,2048]{1,0:T(8,128)(2,1)S(1)} %collective-permute-done.26.refs_0_, bf16[96,2048]{1,0:T(8,128)(2,1)S(1)} %collective-permute-done.27.refs_1_, bf16[2048,768]{1,0:T(8,128)(2,1)S(1)} %bitcast.17, bf16[2048,768]{1,0:T(8,128)(2,1)S(1)} %bitcast.21, ...), custom_call_target="tpu_custom_call" | custom-call | flops 1811939328 | bytes 9437184 | tf_op jit(solution)/shard_map/pallas_call | solution.py:220
  136.4 3.2 %collective-permute-start.32 = (bf16[96,2048]{1,0:T(8,128)(2,1)}, bf16[96,2048]{1,0:T(8,128)(2,1)}, u32[]{:S(2)}, u32[]{:S(2)}) collective-permute-start(bf16[96,2048]{1,0:T(8,128)(2,1)} %get-tuple-element.48), channel_id=1, source_target_pairs={{0,3},{1,0},{2,1},{3,2},{4,7},{5,4},{6,5},{7,6},{8,11},{9,8},{10,9... | collective-permute-start | bytes 1179656 | tf_op jit(solution)/shard_map/ppermute | solution.py:509
  139.6 3.8 %collective-permute-done.21.refs_1_ = bf16[128,2048]{1,0:T(8,128)(2,1)S(1)} collective-permute-done((bf16[128,2048]{1,0:T(8,128)(2,1)S(1)}, bf16[128,2048]{1,0:T(8,128)(2,1)S(1)}, u32[]{:S(2)}, u32[]{:S(2)}) %collective-permute-start.21) | collective-permute-done | bytes 524320 | tf_op jit(solution)/shard_map/ppermute | solution.py:509
  145.4 7.8 %all-to-all-start.1 = ((bf16[64,32,128]{2,1,0:T(8,128)(2,1)}), bf16[64,32,128]{2,1,0:T(8,128)(2,1)}, u32[]{:S(2)}, u32[]{:S(2)}) async-start(bf16[64,32,128]{2,1,0:T(8,128)(2,1)} %bitcast.30), calls=%async_computation.1 | async-start | bytes 1048576 | tf_op jit(solution)/shard_map/all_to_all | solution.py:582
  153.2 1.9 copy-done.3
  155.1 1.9 copy-done.5
  157.0 10.6 %shard_map.155 = (bf16[192,2048]{1,0:T(8,128)(2,1)S(1)}, bf16[96,2048]{1,0:T(8,128)(2,1)S(1)}, bf16[96,2048]{1,0:T(8,128)(2,1)S(1)}, bf16[96,2048]{1,0:T(8,128)(2,1)S(1)}, bf16[96,2048]{1,0:T(8,128)(2,1)S(1)}) custom-call(bf16[192,2048]{1,0:T(8,128)(2,1)} %get-tuple-element.41.refs_0_, bf16[192,2048]{1,0:T(8,128)(2,1)} %collective-permute-done.24.refs_1_, ...), custom_call_target="tpu_custom_call" | custom-call | flops 5435817984 | bytes 9437184 | tf_op jit(solution)/shard_map/pallas_call | solution.py:220
  167.6 3.2 %collective-permute-start.31 = (bf16[96,2048]{1,0:T(8,128)(2,1)S(1)}, bf16[96,2048]{1,0:T(8,128)(2,1)S(1)}, u32[]{:S(2)}, u32[]{:S(2)}) collective-permute-start(bf16[96,2048]{1,0:T(8,128)(2,1)S(1)} %get-tuple-element.46), channel_id=1, source_target_pairs={{0,3},{1,0},{2,1},{3,2},{4,7},{5,4},{6,5},{7,6},{8,11},{9,8},{10,9... | collective-permute-start | bytes 1179656 | tf_op jit(solution)/shard_map/ppermute | solution.py:509
  173.2 3.5 %collective-permute-start.33 = (bf16[96,2048]{1,0:T(8,128)(2,1)S(1)}, bf16[96,2048]{1,0:T(8,128)(2,1)S(1)}, u32[]{:S(2)}, u32[]{:S(2)}) collective-permute-start(bf16[96,2048]{1,0:T(8,128)(2,1)S(1)} %shard_map.158), channel_id=1, source_target_pairs={{0,3},{1,0},{2,1},{3,2},{4,7},{5,4},{6,5},{7,6},{8,11},{9,8},{10,9... | collective-permute-start | bytes 1179656 | tf_op jit(solution)/shard_map/ppermute | solution.py:509
  176.8 4.1 %collective-permute-done.30.refs_2_ = bf16[96,2048]{1,0:T(8,128)(2,1)S(1)} collective-permute-done((bf16[96,2048]{1,0:T(8,128)(2,1)S(1)}, bf16[96,2048]{1,0:T(8,128)(2,1)S(1)}, u32[]{:S(2)}, u32[]{:S(2)}) %collective-permute-start.30) | collective-permute-done | bytes 393248 | tf_op jit(solution)/shard_map/ppermute | solution.py:509
  181.4 7.0 %collective-permute-done.29.refs_1_ = bf16[96,2048]{1,0:T(8,128)(2,1)S(1)} collective-permute-done((bf16[96,2048]{1,0:T(8,128)(2,1)S(1)}, bf16[96,2048]{1,0:T(8,128)(2,1)S(1)}, u32[]{:S(2)}, u32[]{:S(2)}) %collective-permute-start.29) | collective-permute-done | bytes 393248 | tf_op jit(solution)/shard_map/ppermute | solution.py:509
  188.8 1.9 shard_map.159
  190.7 10.3 %all-to-all-start.2 = ((bf16[64,48,128]{2,1,0:T(8,128)(2,1)}), bf16[64,48,128]{2,1,0:T(8,128)(2,1)S(1)}, u32[]{:S(2)}, u32[]{:S(2)}) async-start(bf16[64,48,128]{2,1,0:T(8,128)(2,1)} %bitcast.13), calls=%async_computation.2 | async-start | bytes 1572864 | tf_op jit(solution)/shard_map/all_to_all | solution.py:582
  203.0 9.1 %shard_map.140 = (f32[1024,256]{1,0:T(8,128)S(1)}, f32[1024,128]{1,0:T(8,128)S(1)}, f32[128,128]{1,0:T(8,128)S(1)}) custom-call(f32[2]{0:T(128)S(1)} %copy-done.16, bf16[1024,128]{1,0:T(8,128)(2,1)S(1)} %copy-done.10, bf16[1024,128]{1,0:T(8,128)(2,1)S(1)} %copy-done.11, bf16[1024,256]{1,0:T(8,128)(2,1)S(1)} %copy-done.9, ...), custom_call_target="tpu_custom_call" | custom-call | flops 8000000000 | bytes 4194304 | tf_op jit(solution)/shard_map/pallas_call | solution.py:393
  215.7 3.4 %collective-permute-start.1 = (f32[128,128]{1,0:T(8,128)S(1)}, f32[128,128]{1,0:T(8,128)S(1)}, u32[]{:S(2)}, u32[]{:S(2)}) collective-permute-start(f32[128,128]{1,0:T(8,128)S(1)} %shard_map.141), channel_id=1, source_target_pairs={{0,8},{8,16},{16,24},{24,32},{32,40},{40,48},{48,56},{56,64},{64,7... | collective-permute-start | bytes 196616 | tf_op jit(solution)/shard_map/ppermute | solution.py:596
  219.1 3.0 %collective-permute-done.1.f_ref = f32[128,128]{1,0:T(8,128)S(1)} collective-permute-done((f32[128,128]{1,0:T(8,128)S(1)}, f32[128,128]{1,0:T(8,128)S(1)}, u32[]{:S(2)}, u32[]{:S(2)}) %collective-permute-start.1) | collective-permute-done | bytes 65568 | tf_op jit(solution)/shard_map/ppermute | solution.py:596
  222.1 3.3 %collective-permute-start.2 = (f32[128,128]{1,0:T(8,128)S(1)}, f32[128,128]{1,0:T(8,128)S(1)}, u32[]{:S(2)}, u32[]{:S(2)}) collective-permute-start(f32[128,128]{1,0:T(8,128)S(1)} %collective-permute-done.1.f_ref), channel_id=1, source_target_pairs={{0,8},{8,16},{16,24},{24,32},{32,40},{40,48},{48,56},{56,64},{64,7... | collective-permute-start | bytes 196616 | tf_op jit(solution)/shard_map/ppermute | solution.py:596
  225.4 2.8 collective-permute-done.2.g_ref
  228.8 5.5 %collective-permute-start.3 = (f32[128,128]{1,0:T(8,128)S(1)}, f32[128,128]{1,0:T(8,128)S(1)}, u32[]{:S(2)}, u32[]{:S(2)}) collective-permute-start(f32[128,128]{1,0:T(8,128)S(1)} %shard_map.142.f_ref), channel_id=1, source_target_pairs={{0,16},{8,24},{16,32},{24,40},{32,48},{40,56},{48,64},{56,72},{64,... | collective-permute-start | bytes 196616 | tf_op jit(solution)/shard_map/ppermute | solution.py:596
  234.3 1.9 slice.36
  238.0 2.8 collective-permute-start.13
  241.3 3.2 %collective-permute-start.4 = (f32[128,128]{1,0:T(8,128)S(1)}, f32[128,128]{1,0:T(8,128)S(1)}, u32[]{:S(2)}, u32[]{:S(2)}) collective-permute-start(f32[128,128]{1,0:T(8,128)S(1)} %shard_map.143.f_ref), channel_id=1, source_target_pairs={{0,32},{8,40},{16,48},{24,56},{32,64},{40,72},{48,80},{56,88},{64,... | collective-permute-start | bytes 196616 | tf_op jit(solution)/shard_map/ppermute | solution.py:596
  244.5 1.9 collective-permute-done.4.g_ref
  246.9 6.5 %collective-permute-start.5 = (f32[128,128]{1,0:T(8,128)S(1)}, f32[128,128]{1,0:T(8,128)S(1)}, u32[]{:S(2)}, u32[]{:S(2)}) collective-permute-start(f32[128,128]{1,0:T(8,128)S(1)} %shard_map.144.f_ref), channel_id=1, source_target_pairs={{0,64},{8,72},{16,80},{24,88},{32,96},{40,104},{48,112},{56,120},{... | collective-permute-start | bytes 196616 | tf_op jit(solution)/shard_map/ppermute | solution.py:596
  253.4 1.9 collective-permute-done.5.g_ref
  255.8 9.8 %collective-permute-start.6 = (f32[128,128]{1,0:T(8,128)S(1)}, f32[128,128]{1,0:T(8,128)S(1)}, u32[]{:S(2)}, u32[]{:S(2)}) collective-permute-start(f32[128,128]{1,0:T(8,128)S(1)} %shard_map.145.f_ref), channel_id=1, source_target_pairs={{0,128},{8,136},{16,144},{24,152},{32,160},{40,168},{48,176},{56,1... | collective-permute-start | bytes 196616 | tf_op jit(solution)/shard_map/ppermute | solution.py:596
  265.6 1.9 collective-permute-done.6.l_ref
  269.8 1.8 shard_map.146
  272.5 3.0 %collective-permute-start.8 = (bf16[256,256]{1,0:T(8,128)(2,1)}, bf16[256,256]{1,0:T(8,128)(2,1)S(1)}, u32[]{:S(2)}, u32[]{:S(2)}) collective-permute-start(bf16[256,256]{1,0:T(8,128)(2,1)} %get-tuple-element.31), channel_id=1, source_target_pairs={{0,3},{1,0},{2,1},{3,2},{4,7},{5,4},{6,5},{7,6},{8,11},{9,8},{10,9... | collective-permute-start | bytes 393224 | tf_op jit(solution)/shard_map/ppermute | solution.py:509
  276.8 1.8 collective-permute-done.7.refs_1_
  278.6 3.4 %collective-permute-done.9.refs_3_ = bf16[256,256]{1,0:T(8,128)(2,1)} collective-permute-done((bf16[256,256]{1,0:T(8,128)(2,1)S(1)}, bf16[256,256]{1,0:T(8,128)(2,1)}, u32[]{:S(2)}, u32[]{:S(2)}) %collective-permute-start.9) | collective-permute-done | bytes 131104 | tf_op jit(solution)/shard_map/ppermute | solution.py:509
  283.0 4.7 %shard_map.147 = bf16[256,2048]{1,0:T(8,128)(2,1)} custom-call(bf16[256,256]{1,0:T(8,128)(2,1)S(1)} %copy-done.22, bf16[256,256]{1,0:T(8,128)(2,1)S(1)} %collective-permute-done.7.refs_1_, bf16[256,256]{1,0:T(8,128)(2,1)S(1)} %collective-permute-done.8.refs_2_, bf16[256,256]{1,0:T(8,128)(2,1)} %collective-permute-done.9.refs_3_, ...), custom_call_target="tpu_custom_call" | custom-call | flops 3000000000 | bytes 6000000 | tf_op jit(solution)/shard_map/pallas_call | solution.py:273
  287.6 4.5 %shard_map.160 = bf16[128,2048]{1,0:T(8,128)(2,1)} custom-call(bf16[2048,128]{1,0:T(8,128)(2,1)} %bitcast.12.refs_0_, bf16[3072,128]{1,0:T(8,128)(2,1)S(1)} %bitcast.27, s32[128,2]{1,0:T(8,128)S(1)} %copy.15.r_ref.refs_2_, s32[128,2]{1,0:T(8,128)S(1)} %get-tuple-element.49.refs_3_, f32[128,2]{1,0:T(8,128)S(1)} %copy.17.refs_4_), custom_call_target="tpu_custom_call" | custom-call | flops 335544320 | bytes 1048576 | tf_op jit(solution)/shard_map/pallas_call | solution.py:327
  (110 shorter events, 38.2 us)
Async XLA Ops:
  52.0 39.7 %copy-start = (bf16[1,2048,768]{2,1,0:T(8,128)(2,1)S(1)}, bf16[1,2048,768]{2,1,0:T(8,128)(2,1)}, u32[]{:S(2)}) copy-start(bf16[1,2048,768]{2,1,0:T(8,128)(2,1)} %param.23) | copy-start | bytes 9437188
  54.7 8.1 %collective-permute-start.14 = (bf16[64,2048]{1,0:T(8,128)(2,1)}, bf16[64,2048]{1,0:T(8,128)(2,1)S(1)}, u32[]{:S(2)}, u32[]{:S(2)}) collective-permute-start(bf16[64,2048]{1,0:T(8,128)(2,1)} %get-tuple-element.34.refs_0_), channel_id=1, source_target_pairs={{0,1},{1,2},{2,3},{3,0},{4,5},{5,6},{6,7},{7,4},{8,9},{9,10},{10,1... | collective-permute-start | bytes 786440 | tf_op jit(solution)/shard_map/ppermute | solution.py:509
  56.2 10.8 %collective-permute-start.17 = (bf16[64,2048]{1,0:T(8,128)(2,1)}, bf16[64,2048]{1,0:T(8,128)(2,1)}, u32[]{:S(2)}, u32[]{:S(2)}) collective-permute-start(bf16[64,2048]{1,0:T(8,128)(2,1)} %get-tuple-element.35.refs_1_), channel_id=1, source_target_pairs={{0,3},{1,0},{2,1},{3,2},{4,7},{5,4},{6,5},{7,6},{8,11},{9,8},{10,9... | collective-permute-start | bytes 786440 | tf_op jit(solution)/shard_map/ppermute | solution.py:509
  62.8 10.4 %collective-permute-start.18 = (bf16[64,2048]{1,0:T(8,128)(2,1)S(1)}, bf16[64,2048]{1,0:T(8,128)(2,1)S(1)}, u32[]{:S(2)}, u32[]{:S(2)}) collective-permute-start(bf16[64,2048]{1,0:T(8,128)(2,1)S(1)} %collective-permute-done.14.refs_2_), channel_id=1, source_target_pairs={{0,1},{1,2},{2,3},{3,0},{4,5},{5,6},{6,7},{7,4},{8,9},{9,10},{10,1... | collective-permute-start | bytes 786440 | tf_op jit(solution)/shard_map/ppermute | solution.py:509
  63.8 45.9 %collective-permute-start.24 = (bf16[192,2048]{1,0:T(8,128)(2,1)}, bf16[192,2048]{1,0:T(8,128)(2,1)}, u32[]{:S(2)}, u32[]{:S(2)}) collective-permute-start(bf16[192,2048]{1,0:T(8,128)(2,1)} %get-tuple-element.41.refs_0_), channel_id=1, source_target_pairs={{0,1},{1,2},{2,3},{3,0},{4,5},{5,6},{6,7},{7,4},{8,9},{9,10},{10,1... | collective-permute-start | bytes 2359304 | tf_op jit(solution)/shard_map/ppermute | solution.py:509
  65.3 47.2 %collective-permute-start.25 = (bf16[192,2048]{1,0:T(8,128)(2,1)}, bf16[192,2048]{1,0:T(8,128)(2,1)}, u32[]{:S(2)}, u32[]{:S(2)}) collective-permute-start(bf16[192,2048]{1,0:T(8,128)(2,1)} %get-tuple-element.41.refs_0_), channel_id=1, source_target_pairs={{0,3},{1,0},{2,1},{3,2},{4,7},{5,4},{6,5},{7,6},{8,11},{9,8},{10,9... | collective-permute-start | bytes 2359304 | tf_op jit(solution)/shard_map/ppermute | solution.py:509
  67.0 23.5 %collective-permute-start.19 = (bf16[64,2048]{1,0:T(8,128)(2,1)}, bf16[64,2048]{1,0:T(8,128)(2,1)}, u32[]{:S(2)}, u32[]{:S(2)}) collective-permute-start(bf16[64,2048]{1,0:T(8,128)(2,1)} %collective-permute-done.17.refs_5_), channel_id=1, source_target_pairs={{0,3},{1,0},{2,1},{3,2},{4,7},{5,4},{6,5},{7,6},{8,11},{9,8},{10,9... | collective-permute-start | bytes 786440 | tf_op jit(solution)/shard_map/ppermute | solution.py:509
  68.8 30.4 %collective-permute-start.15 = (bf16[64,2048]{1,0:T(8,128)(2,1)}, bf16[64,2048]{1,0:T(8,128)(2,1)}, u32[]{:S(2)}, u32[]{:S(2)}) collective-permute-start(bf16[64,2048]{1,0:T(8,128)(2,1)} %get-tuple-element.35.refs_1_), channel_id=1, source_target_pairs={{0,1},{1,2},{2,3},{3,0},{4,5},{5,6},{6,7},{7,4},{8,9},{9,10},{10,1... | collective-permute-start | bytes 786440 | tf_op jit(solution)/shard_map/ppermute | solution.py:509
  73.2 28.1 %collective-permute-start.16 = (bf16[64,2048]{1,0:T(8,128)(2,1)}, bf16[64,2048]{1,0:T(8,128)(2,1)}, u32[]{:S(2)}, u32[]{:S(2)}) collective-permute-start(bf16[64,2048]{1,0:T(8,128)(2,1)} %get-tuple-element.34.refs_0_), channel_id=1, source_target_pairs={{0,3},{1,0},{2,1},{3,2},{4,7},{5,4},{6,5},{7,6},{8,11},{9,8},{10,9... | collective-permute-start | bytes 786440 | tf_op jit(solution)/shard_map/ppermute | solution.py:509
  90.5 143.8 %collective-permute-start.10 = (bf16[256,2048]{1,0:T(8,128)(2,1)}, bf16[256,2048]{1,0:T(8,128)(2,1)}, u32[]{:S(2)}, u32[]{:S(2)}) collective-permute-start(bf16[256,2048]{1,0:T(8,128)(2,1)} %refs_4_.2), channel_id=1, source_target_pairs={{0,1},{1,2},{2,3},{3,0},{4,5},{5,6},{6,7},{7,4},{8,9},{9,10},{10,1... | collective-permute-start | bytes 3145736 | tf_op jit(solution)/shard_map/ppermute | solution.py:509
  91.7 1.9 copy-start.1
  93.6 1.9 copy-start.4
  95.5 5.8 %copy-start.2 = (bf16[1,2048,768]{2,1,0:T(8,128)(2,1)S(1)}, bf16[1,2048,768]{2,1,0:T(8,128)(2,1)}, u32[]{:S(2)}) copy-start(bf16[1,2048,768]{2,1,0:T(8,128)(2,1)} %param.24) | copy-start | bytes 9437188
  95.5 5.8 %copy-start.13 = (bf16[64,2048]{1,0:T(8,128)(2,1)S(1)}, bf16[64,2048]{1,0:T(8,128)(2,1)}, u32[]{:S(2)}) copy-start(bf16[64,2048]{1,0:T(8,128)(2,1)} %copy-done.12) | copy-start | bytes 786436
  99.2 16.0 %collective-permute-start.22 = (bf16[64,2048]{1,0:T(8,128)(2,1)S(1)}, bf16[64,2048]{1,0:T(8,128)(2,1)S(1)}, u32[]{:S(2)}, u32[]{:S(2)}) collective-permute-start(bf16[64,2048]{1,0:T(8,128)(2,1)S(1)} %get-tuple-element.40), channel_id=1, source_target_pairs={{0,3},{1,0},{2,1},{3,2},{4,7},{5,4},{6,5},{7,6},{8,11},{9,8},{10,9... | collective-permute-start | bytes 786440 | tf_op jit(solution)/shard_map/ppermute | solution.py:509
  101.3 22.5 %collective-permute-start.20 = (bf16[64,2048]{1,0:T(8,128)(2,1)S(1)}, bf16[64,2048]{1,0:T(8,128)(2,1)S(1)}, u32[]{:S(2)}, u32[]{:S(2)}) collective-permute-start(bf16[64,2048]{1,0:T(8,128)(2,1)S(1)} %get-tuple-element.38), channel_id=1, source_target_pairs={{0,1},{1,2},{2,3},{3,0},{4,5},{5,6},{6,7},{7,4},{8,9},{9,10},{10,1... | collective-permute-start | bytes 786440 | tf_op jit(solution)/shard_map/ppermute | solution.py:509
  110.7 21.4 %collective-permute-start.26 = (bf16[96,2048]{1,0:T(8,128)(2,1)S(1)}, bf16[96,2048]{1,0:T(8,128)(2,1)S(1)}, u32[]{:S(2)}, u32[]{:S(2)}) collective-permute-start(bf16[96,2048]{1,0:T(8,128)(2,1)S(1)} %slice.38), channel_id=1, source_target_pairs={{0,1},{1,2},{2,3},{3,0},{4,5},{5,6},{6,7},{7,4},{8,9},{9,10},{10,1... | collective-permute-start | bytes 1179656 | tf_op jit(solution)/shard_map/ppermute | solution.py:509
  113.5 18.7 %collective-permute-start.27 = (bf16[96,2048]{1,0:T(8,128)(2,1)S(1)}, bf16[96,2048]{1,0:T(8,128)(2,1)S(1)}, u32[]{:S(2)}, u32[]{:S(2)}) collective-permute-start(bf16[96,2048]{1,0:T(8,128)(2,1)S(1)} %slice.39), channel_id=1, source_target_pairs={{0,3},{1,0},{2,1},{3,2},{4,7},{5,4},{6,5},{7,6},{8,11},{9,8},{10,9... | collective-permute-start | bytes 1179656 | tf_op jit(solution)/shard_map/ppermute | solution.py:509
  115.3 24.4 %collective-permute-start.23 = (bf16[128,2048]{1,0:T(8,128)(2,1)S(1)}, bf16[128,2048]{1,0:T(8,128)(2,1)S(1)}, u32[]{:S(2)}, u32[]{:S(2)}) collective-permute-start(bf16[128,2048]{1,0:T(8,128)(2,1)S(1)} %shard_map.153), channel_id=1, source_target_pairs={{0,3},{1,0},{2,1},{3,2},{4,7},{5,4},{6,5},{7,6},{8,11},{9,8},{10,9... | collective-permute-start | bytes 1572872 | tf_op jit(solution)/shard_map/ppermute | solution.py:509
  123.8 19.6 %collective-permute-start.21 = (bf16[128,2048]{1,0:T(8,128)(2,1)S(1)}, bf16[128,2048]{1,0:T(8,128)(2,1)S(1)}, u32[]{:S(2)}, u32[]{:S(2)}) collective-permute-start(bf16[128,2048]{1,0:T(8,128)(2,1)S(1)} %shard_map.152), channel_id=1, source_target_pairs={{0,1},{1,2},{2,3},{3,0},{4,5},{5,6},{6,7},{7,4},{8,9},{9,10},{10,1... | collective-permute-start | bytes 1572872 | tf_op jit(solution)/shard_map/ppermute | solution.py:509
  136.4 34.5 %collective-permute-start.28 = (bf16[96,2048]{1,0:T(8,128)(2,1)}, bf16[96,2048]{1,0:T(8,128)(2,1)}, u32[]{:S(2)}, u32[]{:S(2)}) collective-permute-start(bf16[96,2048]{1,0:T(8,128)(2,1)} %get-tuple-element.44), channel_id=1, source_target_pairs={{0,1},{1,2},{2,3},{3,0},{4,5},{5,6},{6,7},{7,4},{8,9},{9,10},{10,1... | collective-permute-start | bytes 1179656 | tf_op jit(solution)/shard_map/ppermute | solution.py:509
  136.4 35.7 %collective-permute-start.32 = (bf16[96,2048]{1,0:T(8,128)(2,1)}, bf16[96,2048]{1,0:T(8,128)(2,1)}, u32[]{:S(2)}, u32[]{:S(2)}) collective-permute-start(bf16[96,2048]{1,0:T(8,128)(2,1)} %get-tuple-element.48), channel_id=1, source_target_pairs={{0,3},{1,0},{2,1},{3,2},{4,7},{5,4},{6,5},{7,6},{8,11},{9,8},{10,9... | collective-permute-start | bytes 1179656 | tf_op jit(solution)/shard_map/ppermute | solution.py:509
  145.4 45.3 %all-to-all-start.1 = ((bf16[64,32,128]{2,1,0:T(8,128)(2,1)}), bf16[64,32,128]{2,1,0:T(8,128)(2,1)}, u32[]{:S(2)}, u32[]{:S(2)}) async-start(bf16[64,32,128]{2,1,0:T(8,128)(2,1)} %bitcast.30), calls=%async_computation.1 | async-start | bytes 1048576 | tf_op jit(solution)/shard_map/all_to_all | solution.py:582
  153.2 1.9 copy-start.3
  155.1 1.9 copy-start.5
  167.5 13.3 %collective-permute-start.30 = (bf16[96,2048]{1,0:T(8,128)(2,1)S(1)}, bf16[96,2048]{1,0:T(8,128)(2,1)S(1)}, u32[]{:S(2)}, u32[]{:S(2)}) collective-permute-start(bf16[96,2048]{1,0:T(8,128)(2,1)S(1)} %get-tuple-element.45), channel_id=1, source_target_pairs={{0,1},{1,2},{2,3},{3,0},{4,5},{5,6},{6,7},{7,4},{8,9},{9,10},{10,1... | collective-permute-start | bytes 1179656 | tf_op jit(solution)/shard_map/ppermute | solution.py:509
  167.6 13.7 %collective-permute-start.31 = (bf16[96,2048]{1,0:T(8,128)(2,1)S(1)}, bf16[96,2048]{1,0:T(8,128)(2,1)S(1)}, u32[]{:S(2)}, u32[]{:S(2)}) collective-permute-start(bf16[96,2048]{1,0:T(8,128)(2,1)S(1)} %get-tuple-element.46), channel_id=1, source_target_pairs={{0,3},{1,0},{2,1},{3,2},{4,7},{5,4},{6,5},{7,6},{8,11},{9,8},{10,9... | collective-permute-start | bytes 1179656 | tf_op jit(solution)/shard_map/ppermute | solution.py:509
  170.9 10.0 %copy-start.7 = (bf16[256,2048]{1,0:T(8,128)(2,1)S(1)}, bf16[256,2048]{1,0:T(8,128)(2,1)}, u32[]{:S(2)}) copy-start(bf16[256,2048]{1,0:T(8,128)(2,1)} %refs_4_.2) | copy-start | bytes 3145732
  172.0 16.4 %collective-permute-start.29 = (bf16[96,2048]{1,0:T(8,128)(2,1)S(1)}, bf16[96,2048]{1,0:T(8,128)(2,1)S(1)}, u32[]{:S(2)}, u32[]{:S(2)}) collective-permute-start(bf16[96,2048]{1,0:T(8,128)(2,1)S(1)} %shard_map.157), channel_id=1, source_target_pairs={{0,1},{1,2},{2,3},{3,0},{4,5},{5,6},{6,7},{7,4},{8,9},{9,10},{10,1... | collective-permute-start | bytes 1179656 | tf_op jit(solution)/shard_map/ppermute | solution.py:509
  173.2 15.6 %collective-permute-start.33 = (bf16[96,2048]{1,0:T(8,128)(2,1)S(1)}, bf16[96,2048]{1,0:T(8,128)(2,1)S(1)}, u32[]{:S(2)}, u32[]{:S(2)}) collective-permute-start(bf16[96,2048]{1,0:T(8,128)(2,1)S(1)} %shard_map.158), channel_id=1, source_target_pairs={{0,3},{1,0},{2,1},{3,2},{4,7},{5,4},{6,5},{7,6},{8,11},{9,8},{10,9... | collective-permute-start | bytes 1179656 | tf_op jit(solution)/shard_map/ppermute | solution.py:509
  180.8 56.3 %collective-permute-start.11 = (bf16[256,2048]{1,0:T(8,128)(2,1)S(1)}, bf16[256,2048]{1,0:T(8,128)(2,1)S(1)}, u32[]{:S(2)}, u32[]{:S(2)}) collective-permute-start(bf16[256,2048]{1,0:T(8,128)(2,1)S(1)} %copy-done.7), channel_id=1, source_target_pairs={{0,3},{1,0},{2,1},{3,2},{4,7},{5,4},{6,5},{7,6},{8,11},{9,8},{10,9... | collective-permute-start | bytes 3145736 | tf_op jit(solution)/shard_map/ppermute | solution.py:509
  188.8 12.2 %copy-start.10 = (bf16[1024,128]{1,0:T(8,128)(2,1)S(1)}, bf16[1024,128]{1,0:T(8,128)(2,1)}, u32[]{:S(2)}) copy-start(bf16[1024,128]{1,0:T(8,128)(2,1)} %q_ref.1) | copy-start | bytes 786436
  188.8 12.2 %copy-start.16 = (f32[2]{0:T(128)S(1)}, f32[2]{0:T(128)}, u32[]{:S(2)}) copy-start(f32[2]{0:T(128)} %r_ref.2) | copy-start | bytes 28
  190.7 96.9 %all-to-all-start.2 = ((bf16[64,48,128]{2,1,0:T(8,128)(2,1)}), bf16[64,48,128]{2,1,0:T(8,128)(2,1)S(1)}, u32[]{:S(2)}, u32[]{:S(2)}) async-start(bf16[64,48,128]{2,1,0:T(8,128)(2,1)} %bitcast.13), calls=%async_computation.2 | async-start | bytes 1572864 | tf_op jit(solution)/shard_map/all_to_all | solution.py:582
  203.0 64.5 %copy-start.15 = (f32[256]{0:T(256)S(1)}, f32[256]{0:T(256)}, u32[]{:S(2)}) copy-start(f32[256]{0:T(256)} %param.17) | copy-start | bytes 3076
  213.9 1.3 collective-permute-start
  215.7 6.4 %collective-permute-start.1 = (f32[128,128]{1,0:T(8,128)S(1)}, f32[128,128]{1,0:T(8,128)S(1)}, u32[]{:S(2)}, u32[]{:S(2)}) collective-permute-start(f32[128,128]{1,0:T(8,128)S(1)} %shard_map.141), channel_id=1, source_target_pairs={{0,8},{8,16},{16,24},{24,32},{32,40},{40,48},{48,56},{56,64},{64,7... | collective-permute-start | bytes 196616 | tf_op jit(solution)/shard_map/ppermute | solution.py:596
  222.1 6.1 %collective-permute-start.2 = (f32[128,128]{1,0:T(8,128)S(1)}, f32[128,128]{1,0:T(8,128)S(1)}, u32[]{:S(2)}, u32[]{:S(2)}) collective-permute-start(f32[128,128]{1,0:T(8,128)S(1)} %collective-permute-done.1.f_ref), channel_id=1, source_target_pairs={{0,8},{8,16},{16,24},{24,32},{32,40},{40,48},{48,56},{56,64},{64,7... | collective-permute-start | bytes 196616 | tf_op jit(solution)/shard_map/ppermute | solution.py:596
  228.8 12.0 %collective-permute-start.3 = (f32[128,128]{1,0:T(8,128)S(1)}, f32[128,128]{1,0:T(8,128)S(1)}, u32[]{:S(2)}, u32[]{:S(2)}) collective-permute-start(f32[128,128]{1,0:T(8,128)S(1)} %shard_map.142.f_ref), channel_id=1, source_target_pairs={{0,16},{8,24},{16,32},{24,40},{32,48},{40,56},{48,64},{56,72},{64,... | collective-permute-start | bytes 196616 | tf_op jit(solution)/shard_map/ppermute | solution.py:596
  236.2 45.9 %collective-permute-start.12 = (bf16[128,2048]{1,0:T(8,128)(2,1)}, bf16[128,2048]{1,0:T(8,128)(2,1)}, u32[]{:S(2)}, u32[]{:S(2)}) collective-permute-start(bf16[128,2048]{1,0:T(8,128)(2,1)} %slice.36), channel_id=1, source_target_pairs={{0,1},{1,2},{2,3},{3,0},{4,5},{5,6},{6,7},{7,4},{8,9},{9,10},{10,1... | collective-permute-start | bytes 1572872 | tf_op jit(solution)/shard_map/ppermute | solution.py:509
  238.0 44.1 %collective-permute-start.13 = (bf16[128,2048]{1,0:T(8,128)(2,1)}, bf16[128,2048]{1,0:T(8,128)(2,1)}, u32[]{:S(2)}, u32[]{:S(2)}) collective-permute-start(bf16[128,2048]{1,0:T(8,128)(2,1)} %slice.37), channel_id=1, source_target_pairs={{0,3},{1,0},{2,1},{3,2},{4,7},{5,4},{6,5},{7,6},{8,11},{9,8},{10,9... | collective-permute-start | bytes 1572872 | tf_op jit(solution)/shard_map/ppermute | solution.py:509
  241.3 5.1 %collective-permute-start.4 = (f32[128,128]{1,0:T(8,128)S(1)}, f32[128,128]{1,0:T(8,128)S(1)}, u32[]{:S(2)}, u32[]{:S(2)}) collective-permute-start(f32[128,128]{1,0:T(8,128)S(1)} %shard_map.143.f_ref), channel_id=1, source_target_pairs={{0,32},{8,40},{16,48},{24,56},{32,64},{40,72},{48,80},{56,88},{64,... | collective-permute-start | bytes 196616 | tf_op jit(solution)/shard_map/ppermute | solution.py:596
  246.9 8.3 %collective-permute-start.5 = (f32[128,128]{1,0:T(8,128)S(1)}, f32[128,128]{1,0:T(8,128)S(1)}, u32[]{:S(2)}, u32[]{:S(2)}) collective-permute-start(f32[128,128]{1,0:T(8,128)S(1)} %shard_map.144.f_ref), channel_id=1, source_target_pairs={{0,64},{8,72},{16,80},{24,88},{32,96},{40,104},{48,112},{56,120},{... | collective-permute-start | bytes 196616 | tf_op jit(solution)/shard_map/ppermute | solution.py:596
  255.8 11.7 %collective-permute-start.6 = (f32[128,128]{1,0:T(8,128)S(1)}, f32[128,128]{1,0:T(8,128)S(1)}, u32[]{:S(2)}, u32[]{:S(2)}) collective-permute-start(f32[128,128]{1,0:T(8,128)S(1)} %shard_map.145.f_ref), channel_id=1, source_target_pairs={{0,128},{8,136},{16,144},{24,152},{32,160},{40,168},{48,176},{56,1... | collective-permute-start | bytes 196616 | tf_op jit(solution)/shard_map/ppermute | solution.py:596
  269.8 6.9 %copy-start.23 = (f32[128,2]{0,1:T(2,128)S(1)}, f32[128,2]{0,1:T(2,128)}, u32[]{:S(2)}) copy-start(f32[128,2]{0,1:T(2,128)} %param.22) | copy-start | bytes 3076
  272.2 6.4 %collective-permute-start.7 = (bf16[256,256]{1,0:T(8,128)(2,1)}, bf16[256,256]{1,0:T(8,128)(2,1)S(1)}, u32[]{:S(2)}, u32[]{:S(2)}) collective-permute-start(bf16[256,256]{1,0:T(8,128)(2,1)} %get-tuple-element.30), channel_id=1, source_target_pairs={{0,1},{1,2},{2,3},{3,0},{4,5},{5,6},{6,7},{7,4},{8,9},{9,10},{10,1... | collective-permute-start | bytes 393224 | tf_op jit(solution)/shard_map/ppermute | solution.py:509
  272.5 6.2 %collective-permute-start.8 = (bf16[256,256]{1,0:T(8,128)(2,1)}, bf16[256,256]{1,0:T(8,128)(2,1)S(1)}, u32[]{:S(2)}, u32[]{:S(2)}) collective-permute-start(bf16[256,256]{1,0:T(8,128)(2,1)} %get-tuple-element.31), channel_id=1, source_target_pairs={{0,3},{1,0},{2,1},{3,2},{4,7},{5,4},{6,5},{7,6},{8,11},{9,8},{10,9... | collective-permute-start | bytes 393224 | tf_op jit(solution)/shard_map/ppermute | solution.py:509
  275.5 6.6 %collective-permute-start.9 = (bf16[256,256]{1,0:T(8,128)(2,1)S(1)}, bf16[256,256]{1,0:T(8,128)(2,1)}, u32[]{:S(2)}, u32[]{:S(2)}) collective-permute-start(bf16[256,256]{1,0:T(8,128)(2,1)S(1)} %get-tuple-element.32), channel_id=1, source_target_pairs={{0,2},{1,3},{2,0},{3,1},{4,6},{5,7},{6,4},{7,5},{8,10},{9,11},{10,... | collective-permute-start | bytes 393224 | tf_op jit(solution)/shard_map/ppermute | solution.py:509
  (12 other events, 10.8 us)
where the time goes:
time: 297 us; the launch traced here: 292 us
  starting transfers between devices  86.6 us (29%)
  waiting for transfers between devices  73.3 us (25%)
  Pallas kernels  60.3 us (20%)
  blocking collectives  46.3 us (16%)
  local copies, waits for them, and re-layouts  24 us (8%)
    ppermute x27, waiting for transfers between devices, send(): return lax.ppermute(x, 'tp', to)  60.8 us
    all_to_all x1, blocking collectives, program(): lax.all_to_all(sent.reshape(experts, cap * cuts, LANES), EP, split_axis=0...  46.3 us
    ppermute x27, starting transfers between devices, send(): return lax.ppermute(x, 'tp', to)  36.8 us
    ppermute x6, starting transfers between devices, ahead(): return lax.ppermute(x, EP[:2], [(i, i + k) for i in range(chips - k)])  31.6 us
    pallas_call x4, Pallas kernels, expert(): pl.pallas_call(body, grid=(steps,), in_specs=[whole(size) for size in siz...  26.8 us
    unnamed x50, local copies, waits for them, and re-layouts  19.2 us
    all_to_all x2, starting transfers between devices, program(): lax.all_to_all(packed.reshape(experts, count * cuts, LANES), EP, split_ax...  18.1 us
    ppermute x6, waiting for transfers between devices, ahead(): return lax.ppermute(x, EP[:2], [(i, i + k) for i in range(chips - k)])  11.5 us
  transfers between devices with their start and end apart: 36, of which 17 were waited for; matrix products, arithmetic and copies ran while one was open for 2% of the time, Pallas kernels for 17%

commit v1 on v0

--- a/solution.py
+++ b/solution.py
@@ -105,9 +105,11 @@
     )(x, gain.reshape(1, width), routes)
 
 
-def unpack(lines, width, groups, cap):
+def unpack(lines, width, groups, cap, n):
     cuts = width // LANES
     half = groups // 2
+    first, count = SLOTS[n]
+    apart = n < len(SLOTS) - 1
 
     def body(x_ref, *refs):
         outs, scr = refs[:-1], refs[-1]
@@ -116,19 +118,18 @@
         @pl.loop(0, cuts)
         def _(c):
             cols = pl.ds(pl.multiple_of(c * LANES, LANES), LANES)
-            for n, (first, count) in enumerate(SLOTS):
-                for side in range(2):
-                    for s in range(count):
-                        start = side * half * cap * cuts + (first + s) * cuts + c
-                        row = (n * side * count + s) * half
-                        outs[2 if n else side][row : row + half, cols] = scr[
-                            pl.ds(start, half, stride=cap * cuts), :
-                        ].astype(BF16)
-
-    near, late = (count * half for _, count in SLOTS)
-    return pl.pallas_call(
-        body,
-        out_shape=[jax.ShapeDtypeStruct((size, width), BF16) for size in (near, near, 2 * late)],
+            for side in range(2):
+                for s in range(count):
+                    start = side * half * cap * cuts + (first + s) * cuts + c
+                    out, row = (outs[side], s) if apart else (outs[0], side * count + s)
+                    out[row * half : (row + 1) * half, cols] = scr[
+                        pl.ds(start, half, stride=cap * cuts), :
+                    ].astype(BF16)
+
+    sizes = [count * half] * 2 if apart else [2 * count * half]
+    return pl.pallas_call(
+        body,
+        out_shape=[jax.ShapeDtypeStruct((size, width), BF16) for size in sizes],
         scratch_shapes=[pltpu.VMEM(lines.shape, F32)],
         compiler_params=params(16),
         cost_estimate=cost(2e9, 4 * lines.size),
@@ -239,12 +240,20 @@
 
 def add(whole, term, first):
     rows = term.shape[0]
+    others = [n for n in range(0, whole.shape[0], rows) if n != first]
+    step = 32
 
     def body(a_ref, b_ref, o_ref):
-        if rows < whole.shape[0]:
-            o_ref[...] = a_ref[...]
-        at = slice(first, first + rows)
-        o_ref[at, :] = (a_ref[at, :].astype(F32) + b_ref[...].astype(F32)).astype(BF16)
+        @pl.loop(0, rows // step)
+        def _(n):
+            row = pl.multiple_of(n * step, step)
+            at = pl.ds(first + row, step)
+            o_ref[at, :] = (
+                a_ref[at, :].astype(F32) + b_ref[pl.ds(row, step), :].astype(F32)
+            ).astype(BF16)
+            for other in others:
+                same = pl.ds(other + row, step)
+                o_ref[same, :] = a_ref[same, :]
 
     return pl.pallas_call(
         body,
@@ -454,15 +463,21 @@
         c = at_ref[2]
         me = at_ref[3]
         past = f_ref[...] + l_ref[...] * falls(r_ref, heads, float(spans))
-        st[...] = jnp.where(c == 1, o_ref[...], 0.0) + past * falls(r_ref, heads, c.astype(F32))
+        past = jnp.where(c == 1, o_ref[...], 0.0) + past * falls(r_ref, heads, c.astype(F32))
+        st[...] = jnp.zeros((heads * DK, wide), F32)
+        for h in range(heads):
+            keys = slice(h * DK, (h + 1) * DK)
+            st[keys, h * DV : (h + 1) * DV] = past[keys, :]
+        high, low = split(st[...])
         for away, out in zip((0, 1, 3, 2), outs):
             block = lax.rem(me + away, tensor)
             rows = pl.ds(pl.multiple_of(block * share, share), share)
+            q_high, q_low = split(q_ref[rows, :])
+            terms = ((q_high, high), (q_high, low), (q_low, high))
+            cross = sum(jnp.dot(a, b, preferred_element_type=F32) for a, b in terms)
             for h in range(heads):
                 cols = slice(h * DV, (h + 1) * DV)
-                ret = y_ref[rows, cols] + product(
-                    q_ref[rows, h * DK : (h + 1) * DK], st[h * DK : (h + 1) * DK, :], PLAIN
-                )
+                ret = y_ref[rows, cols] + cross[:, cols]
                 mean_sq = jnp.mean(ret * ret, axis=-1, keepdims=True)
                 out[:, cols] = (ret * lax.rsqrt(mean_sq + EPS) * g_ref[:, cols]).astype(BF16)
 
@@ -470,7 +485,7 @@
         body,
         in_specs=[SMEM, SMEM] + [pl.BlockSpec()] * 6,
         out_shape=[jax.ShapeDtypeStruct((share, wide), BF16)] * tensor,
-        scratch_shapes=[pltpu.VMEM((heads * DK, DV), F32)],
+        scratch_shapes=[pltpu.VMEM((heads * DK, wide), F32)],
         compiler_params=params(),
         cost_estimate=cost(2e9, 8 * span * wide),
     )(rate, at, inner, q_fallen, other, far, got, gain.reshape(1, wide))
@@ -536,7 +551,9 @@
     arrived = lax.all_to_all(
         sent.reshape(experts, cap * cuts, LANES), EP, split_axis=0, concat_axis=0, tiled=True
     )
-    owns = unpack(arrived.reshape(-1, LANES), width, groups, cap)
+    arrived = arrived.reshape(-1, LANES)
+    owns = unpack(arrived, width, groups, cap, 0)
+    owns += unpack(arrived, width, groups, cap, 1)
 
     answers = []
     for n, (_, count) in enumerate(SLOTS):

time: 297 us -> 304 us (1.024)
  starting transfers between devices: 86.6 us -> 90.1 us
  waiting for transfers between devices: 73.3 us -> 76.5 us
    ppermute x27, waiting for transfers between devices: 60.8 us -> 64 us  [send(): return lax.ppermute(x, 'tp', to)]
  transfers between devices with their start and end apart: 36 -> 36, of which waited for: 17 -> 17; matrix products, arithmetic and copies ran while one was open for 2% -> 2% of each run, Pallas kernels for 17% -> 18%
where the time goes in v1:
time: 304 us; the launch traced here: 299 us
  starting transfers between devices  90.1 us (30%)
  waiting for transfers between devices  76.5 us (25%)
  Pallas kernels  61.4 us (20%)
  blocking collectives  46.3 us (15%)
  local copies, waits for them, and re-layouts  23.4 us (8%)
    ppermute x27, waiting for transfers between devices, send(): return lax.ppermute(x, 'tp', to)  64 us
    all_to_all x1, blocking collectives, program(): lax.all_to_all(sent.reshape(experts, cap * cuts, LANES), EP, split_axis=0...  46.3 us
    ppermute x27, starting transfers between devices, send(): return lax.ppermute(x, 'tp', to)  37.3 us
    ppermute x6, starting transfers between devices, ahead(): return lax.ppermute(x, EP[:2], [(i, i + k) for i in range(chips - k)])  31.6 us
    pallas_call x4, Pallas kernels, expert(): pl.pallas_call(body, grid=(steps,), in_specs=[whole(size) for size in siz...  26.8 us
    all_to_all x2, starting transfers between devices, program(): lax.all_to_all(packed.reshape(experts, count * cuts, LANES), EP, split_ax...  21.1 us
    unnamed x50, local copies, waits for them, and re-layouts  18.6 us
    ppermute x6, waiting for transfers between devices, ahead(): return lax.ppermute(x, EP[:2], [(i, i + k) for i in range(chips - k)])  11.5 us
  transfers between devices with their start and end apart: 36, of which 17 were waited for; matrix products, arithmetic and copies ran while one was open for 2% of the time, Pallas kernels for 18%

profile of v1, /device:TPU:8, one launch (start us, length us, event | category | flops | bytes accessed | tf_op | source)
XLA Modules:
  0.0 299.1 jit_solution(1308596989739860977)
XLA Ops:
  3.2 2.6 shard_map.148
  5.7 46.3 %all_to_all.15 = bf16[64,80,128]{2,1,0:T(8,128)(2,1)S(1)} all-to-all(bf16[64,80,128]{2,1,0:T(8,128)(2,1)S(1)} %bitcast.30), channel_id=1, replica_groups=mesh['ep_0'=8,'ep_1'=4,'ep_2'=2,'tp'=4] {'ep_0','ep_1','ep_2'}, dimensions={0} | all-to-all | bytes 2621440 | tf_op jit(solution)/shard_map/all_to_all | solution.py:551
  56.9 4.9 %collective-permute-done.14.refs_2_ = bf16[64,2048]{1,0:T(8,128)(2,1)S(1)} collective-permute-done((bf16[64,2048]{1,0:T(8,128)(2,1)}, bf16[64,2048]{1,0:T(8,128)(2,1)S(1)}, u32[]{:S(2)}, u32[]{:S(2)}) %collective-permute-start.14) | collective-permute-done | bytes 262176 | tf_op jit(solution)/shard_map/ppermute | solution.py:524
  63.5 1.8 collective-permute-start.16
  67.0 2.0 shard_map.155.refs_0_
  69.3 2.9 collective-permute-done.18.refs_0_
  72.5 6.1 %collective-permute-done.19.refs_1_ = bf16[64,2048]{1,0:T(8,128)(2,1)} collective-permute-done((bf16[64,2048]{1,0:T(8,128)(2,1)}, bf16[64,2048]{1,0:T(8,128)(2,1)}, u32[]{:S(2)}, u32[]{:S(2)}) %collective-permute-start.19) | collective-permute-done | bytes 262176 | tf_op jit(solution)/shard_map/ppermute | solution.py:524
  79.8 1.9 copy-done.1
  81.7 1.9 copy-done.4
  83.6 3.7 %shard_map.151 = (bf16[64,2048]{1,0:T(8,128)(2,1)S(1)}, bf16[64,2048]{1,0:T(8,128)(2,1)S(1)}) custom-call(bf16[64,2048]{1,0:T(8,128)(2,1)S(1)} %collective-permute-done.18.refs_0_, bf16[64,2048]{1,0:T(8,128)(2,1)} %collective-permute-done.19.refs_1_, bf16[2048,768]{1,0:T(8,128)(2,1)S(1)} %bitcast.15, bf16[2048,768]{1,0:T(8,128)(2,1)S(1)} %bitcast.19, ...), custom_call_target="tpu_custom_call" | custom-call | flops 1207959552 | bytes 9437184 | tf_op jit(solution)/shard_map/pallas_call | solution.py:221
  87.3 2.1 collective-permute-start.22
  89.4 8.4 %shard_map.150 = (bf16[128,2048]{1,0:T(8,128)(2,1)S(1)}, bf16[128,2048]{1,0:T(8,128)(2,1)S(1)}, bf16[128,2048]{1,0:T(8,128)(2,1)S(1)}) custom-call(bf16[64,2048]{1,0:T(8,128)(2,1)} %get-tuple-element.33.refs_0_, bf16[64,2048]{1,0:T(8,128)(2,1)} %get-tuple-element.34.refs_1_, bf16[64,2048]{1,0:T(8,128)(2,1)S(1)} %copy-done.13, ...), custom_call_target="tpu_custom_call" | custom-call | flops 3623878656 | bytes 9437184 | tf_op jit(solution)/shard_map/pallas_call | solution.py:221
  98.1 3.1 %collective-permute-start.23 = (bf16[128,2048]{1,0:T(8,128)(2,1)S(1)}, bf16[128,2048]{1,0:T(8,128)(2,1)S(1)}, u32[]{:S(2)}, u32[]{:S(2)}) collective-permute-start(bf16[128,2048]{1,0:T(8,128)(2,1)S(1)} %shard_map.153), channel_id=1, source_target_pairs={{0,3},{1,0},{2,1},{3,2},{4,7},{5,4},{6,5},{7,6},{8,11},{9,8},{10,9... | collective-permute-start | bytes 1572872 | tf_op jit(solution)/shard_map/ppermute | solution.py:524
  101.2 18.2 %collective-permute-done.20.b_ref = bf16[64,2048]{1,0:T(8,128)(2,1)S(1)} collective-permute-done((bf16[64,2048]{1,0:T(8,128)(2,1)S(1)}, bf16[64,2048]{1,0:T(8,128)(2,1)S(1)}, u32[]{:S(2)}, u32[]{:S(2)}) %collective-permute-start.20) | collective-permute-done | bytes 262176 | tf_op jit(solution)/shard_map/ppermute | solution.py:524
  122.6 2.4 collective-permute-start.27
  125.4 14.5 %collective-permute-done.26.refs_0_ = bf16[96,2048]{1,0:T(8,128)(2,1)S(1)} collective-permute-done((bf16[96,2048]{1,0:T(8,128)(2,1)S(1)}, bf16[96,2048]{1,0:T(8,128)(2,1)S(1)}, u32[]{:S(2)}, u32[]{:S(2)}) %collective-permute-start.26) | collective-permute-done | bytes 393248 | tf_op jit(solution)/shard_map/ppermute | solution.py:524
  139.8 4.2 %shard_map.157 = (bf16[96,2048]{1,0:T(8,128)(2,1)}, bf16[96,2048]{1,0:T(8,128)(2,1)}) custom-call(bf16[96,2048]{1,0:T(8,128)(2,1)S(1)} %collective-permute-done.26.refs_0_, bf16[96,2048]{1,0:T(8,128)(2,1)S(1)} %collective-permute-done.27.refs_1_, bf16[2048,768]{1,0:T(8,128)(2,1)S(1)} %bitcast.17, bf16[2048,768]{1,0:T(8,128)(2,1)S(1)} %bitcast.21, ...), custom_call_target="tpu_custom_call" | custom-call | flops 1811939328 | bytes 9437184 | tf_op jit(solution)/shard_map/pallas_call | solution.py:221
  144.1 3.2 %collective-permute-start.32 = (bf16[96,2048]{1,0:T(8,128)(2,1)}, bf16[96,2048]{1,0:T(8,128)(2,1)}, u32[]{:S(2)}, u32[]{:S(2)}) collective-permute-start(bf16[96,2048]{1,0:T(8,128)(2,1)} %get-tuple-element.46), channel_id=1, source_target_pairs={{0,3},{1,0},{2,1},{3,2},{4,7},{5,4},{6,5},{7,6},{8,11},{9,8},{10,9... | collective-permute-start | bytes 1179656 | tf_op jit(solution)/shard_map/ppermute | solution.py:524
  149.3 10.8 %all-to-all-start.1 = ((bf16[64,32,128]{2,1,0:T(8,128)(2,1)}), bf16[64,32,128]{2,1,0:T(8,128)(2,1)}, u32[]{:S(2)}, u32[]{:S(2)}) async-start(bf16[64,32,128]{2,1,0:T(8,128)(2,1)} %bitcast.31), calls=%async_computation.1 | async-start | bytes 1048576 | tf_op jit(solution)/shard_map/all_to_all | solution.py:599
  160.1 1.9 copy-done.3
  161.9 1.9 copy-done.5
  163.8 10.6 %shard_map.156 = (bf16[192,2048]{1,0:T(8,128)(2,1)S(1)}, bf16[96,2048]{1,0:T(8,128)(2,1)S(1)}, bf16[96,2048]{1,0:T(8,128)(2,1)S(1)}, bf16[96,2048]{1,0:T(8,128)(2,1)S(1)}, bf16[96,2048]{1,0:T(8,128)(2,1)S(1)}) custom-call(bf16[192,2048]{1,0:T(8,128)(2,1)} %shard_map.155.refs_0_, bf16[192,2048]{1,0:T(8,128)(2,1)} %collective-permute-done.24.refs_1_, ...), custom_call_target="tpu_custom_call" | custom-call | flops 5435817984 | bytes 9437184 | tf_op jit(solution)/shard_map/pallas_call | solution.py:221
  174.5 3.2 %collective-permute-start.31 = (bf16[96,2048]{1,0:T(8,128)(2,1)S(1)}, bf16[96,2048]{1,0:T(8,128)(2,1)S(1)}, u32[]{:S(2)}, u32[]{:S(2)}) collective-permute-start(bf16[96,2048]{1,0:T(8,128)(2,1)S(1)} %get-tuple-element.44), channel_id=1, source_target_pairs={{0,3},{1,0},{2,1},{3,2},{4,7},{5,4},{6,5},{7,6},{8,11},{9,8},{10,9... | collective-permute-start | bytes 1179656 | tf_op jit(solution)/shard_map/ppermute | solution.py:524
  180.1 3.5 %collective-permute-start.33 = (bf16[96,2048]{1,0:T(8,128)(2,1)S(1)}, bf16[96,2048]{1,0:T(8,128)(2,1)S(1)}, u32[]{:S(2)}, u32[]{:S(2)}) collective-permute-start(bf16[96,2048]{1,0:T(8,128)(2,1)S(1)} %shard_map.159), channel_id=1, source_target_pairs={{0,3},{1,0},{2,1},{3,2},{4,7},{5,4},{6,5},{7,6},{8,11},{9,8},{10,9... | collective-permute-start | bytes 1179656 | tf_op jit(solution)/shard_map/ppermute | solution.py:524
  183.7 4.0 %collective-permute-done.30.refs_2_ = bf16[96,2048]{1,0:T(8,128)(2,1)S(1)} collective-permute-done((bf16[96,2048]{1,0:T(8,128)(2,1)S(1)}, bf16[96,2048]{1,0:T(8,128)(2,1)S(1)}, u32[]{:S(2)}, u32[]{:S(2)}) %collective-permute-start.30) | collective-permute-done | bytes 393248 | tf_op jit(solution)/shard_map/ppermute | solution.py:524
  187.7 7.6 %collective-permute-done.29.refs_1_ = bf16[96,2048]{1,0:T(8,128)(2,1)S(1)} collective-permute-done((bf16[96,2048]{1,0:T(8,128)(2,1)S(1)}, bf16[96,2048]{1,0:T(8,128)(2,1)S(1)}, u32[]{:S(2)}, u32[]{:S(2)}) %collective-permute-start.29) | collective-permute-done | bytes 393248 | tf_op jit(solution)/shard_map/ppermute | solution.py:524
  195.7 1.9 shard_map.160
  197.6 10.3 %all-to-all-start.2 = ((bf16[64,48,128]{2,1,0:T(8,128)(2,1)}), bf16[64,48,128]{2,1,0:T(8,128)(2,1)S(1)}, u32[]{:S(2)}, u32[]{:S(2)}) async-start(bf16[64,48,128]{2,1,0:T(8,128)(2,1)} %bitcast.13), calls=%async_computation.2 | async-start | bytes 1572864 | tf_op jit(solution)/shard_map/all_to_all | solution.py:599
  209.9 9.1 %shard_map.140 = (f32[1024,256]{1,0:T(8,128)S(1)}, f32[1024,128]{1,0:T(8,128)S(1)}, f32[128,128]{1,0:T(8,128)S(1)}) custom-call(f32[2]{0:T(128)S(1)} %copy-done.16, bf16[1024,128]{1,0:T(8,128)(2,1)S(1)} %copy-done.10, bf16[1024,128]{1,0:T(8,128)(2,1)S(1)} %copy-done.11, bf16[1024,256]{1,0:T(8,128)(2,1)S(1)} %copy-done.9, ...), custom_call_target="tpu_custom_call" | custom-call | flops 8000000000 | bytes 4194304 | tf_op jit(solution)/shard_map/pallas_call | solution.py:402
  222.5 3.4 %collective-permute-start.1 = (f32[128,128]{1,0:T(8,128)S(1)}, f32[128,128]{1,0:T(8,128)S(1)}, u32[]{:S(2)}, u32[]{:S(2)}) collective-permute-start(f32[128,128]{1,0:T(8,128)S(1)} %shard_map.141), channel_id=1, source_target_pairs={{0,8},{8,16},{16,24},{24,32},{32,40},{40,48},{48,56},{56,64},{64,7... | collective-permute-start | bytes 196616 | tf_op jit(solution)/shard_map/ppermute | solution.py:613
  225.9 3.0 collective-permute-done.1.f_ref
  228.9 3.3 %collective-permute-start.2 = (f32[128,128]{1,0:T(8,128)S(1)}, f32[128,128]{1,0:T(8,128)S(1)}, u32[]{:S(2)}, u32[]{:S(2)}) collective-permute-start(f32[128,128]{1,0:T(8,128)S(1)} %collective-permute-done.1.f_ref), channel_id=1, source_target_pairs={{0,8},{8,16},{16,24},{24,32},{32,40},{40,48},{48,56},{56,64},{64,7... | collective-permute-start | bytes 196616 | tf_op jit(solution)/shard_map/ppermute | solution.py:613
  232.2 2.8 collective-permute-done.2.g_ref
  235.6 5.5 %collective-permute-start.3 = (f32[128,128]{1,0:T(8,128)S(1)}, f32[128,128]{1,0:T(8,128)S(1)}, u32[]{:S(2)}, u32[]{:S(2)}) collective-permute-start(f32[128,128]{1,0:T(8,128)S(1)} %shard_map.142.f_ref), channel_id=1, source_target_pairs={{0,16},{8,24},{16,32},{24,40},{32,48},{40,56},{48,64},{56,72},{64,... | collective-permute-start | bytes 196616 | tf_op jit(solution)/shard_map/ppermute | solution.py:613
  241.1 1.9 slice.36
  243.9 3.7 %collective-permute-start.13 = (bf16[128,2048]{1,0:T(8,128)(2,1)}, bf16[128,2048]{1,0:T(8,128)(2,1)}, u32[]{:S(2)}, u32[]{:S(2)}) collective-permute-start(bf16[128,2048]{1,0:T(8,128)(2,1)} %slice.37), channel_id=1, source_target_pairs={{0,3},{1,0},{2,1},{3,2},{4,7},{5,4},{6,5},{7,6},{8,11},{9,8},{10,9... | collective-permute-start | bytes 1572872 | tf_op jit(solution)/shard_map/ppermute | solution.py:524
  248.2 3.2 %collective-permute-start.4 = (f32[128,128]{1,0:T(8,128)S(1)}, f32[128,128]{1,0:T(8,128)S(1)}, u32[]{:S(2)}, u32[]{:S(2)}) collective-permute-start(f32[128,128]{1,0:T(8,128)S(1)} %shard_map.143.f_ref), channel_id=1, source_target_pairs={{0,32},{8,40},{16,48},{24,56},{32,64},{40,72},{48,80},{56,88},{64,... | collective-permute-start | bytes 196616 | tf_op jit(solution)/shard_map/ppermute | solution.py:613
  251.4 1.9 collective-permute-done.4.g_ref
  253.8 6.5 %collective-permute-start.5 = (f32[128,128]{1,0:T(8,128)S(1)}, f32[128,128]{1,0:T(8,128)S(1)}, u32[]{:S(2)}, u32[]{:S(2)}) collective-permute-start(f32[128,128]{1,0:T(8,128)S(1)} %shard_map.144.f_ref), channel_id=1, source_target_pairs={{0,64},{8,72},{16,80},{24,88},{32,96},{40,104},{48,112},{56,120},{... | collective-permute-start | bytes 196616 | tf_op jit(solution)/shard_map/ppermute | solution.py:613
  260.3 1.9 collective-permute-done.5.g_ref
  262.7 9.8 %collective-permute-start.6 = (f32[128,128]{1,0:T(8,128)S(1)}, f32[128,128]{1,0:T(8,128)S(1)}, u32[]{:S(2)}, u32[]{:S(2)}) collective-permute-start(f32[128,128]{1,0:T(8,128)S(1)} %shard_map.145.f_ref), channel_id=1, source_target_pairs={{0,128},{8,136},{16,144},{24,152},{32,160},{40,168},{48,176},{56,1... | collective-permute-start | bytes 196616 | tf_op jit(solution)/shard_map/ppermute | solution.py:613
  272.5 1.9 collective-permute-done.6.l_ref
  276.6 1.9 shard_map.146
  279.2 3.2 %collective-permute-start.8 = (bf16[256,256]{1,0:T(8,128)(2,1)}, bf16[256,256]{1,0:T(8,128)(2,1)S(1)}, u32[]{:S(2)}, u32[]{:S(2)}) collective-permute-start(bf16[256,256]{1,0:T(8,128)(2,1)} %get-tuple-element.30), channel_id=1, source_target_pairs={{0,3},{1,0},{2,1},{3,2},{4,7},{5,4},{6,5},{7,6},{8,11},{9,8},{10,9... | collective-permute-start | bytes 393224 | tf_op jit(solution)/shard_map/ppermute | solution.py:524
  283.8 1.8 collective-permute-done.7.refs_1_
  285.6 3.4 %collective-permute-done.9.refs_3_ = bf16[256,256]{1,0:T(8,128)(2,1)} collective-permute-done((bf16[256,256]{1,0:T(8,128)(2,1)S(1)}, bf16[256,256]{1,0:T(8,128)(2,1)}, u32[]{:S(2)}, u32[]{:S(2)}) %collective-permute-start.9) | collective-permute-done | bytes 131104 | tf_op jit(solution)/shard_map/ppermute | solution.py:524
  290.0 4.7 %shard_map.147 = bf16[256,2048]{1,0:T(8,128)(2,1)} custom-call(bf16[256,256]{1,0:T(8,128)(2,1)S(1)} %copy-done.22, bf16[256,256]{1,0:T(8,128)(2,1)S(1)} %collective-permute-done.7.refs_1_, bf16[256,256]{1,0:T(8,128)(2,1)S(1)} %collective-permute-done.8.refs_2_, bf16[256,256]{1,0:T(8,128)(2,1)} %collective-permute-done.9.refs_3_, ...), custom_call_target="tpu_custom_call" | custom-call | flops 3000000000 | bytes 6000000 | tf_op jit(solution)/shard_map/pallas_call | solution.py:282
  294.6 4.5 %shard_map.161 = bf16[128,2048]{1,0:T(8,128)(2,1)} custom-call(bf16[2048,128]{1,0:T(8,128)(2,1)} %bitcast.12.refs_0_, bf16[3072,128]{1,0:T(8,128)(2,1)S(1)} %bitcast.27, s32[128,2]{1,0:T(8,128)S(1)} %copy.15.r_ref.refs_2_, s32[128,2]{1,0:T(8,128)S(1)} %get-tuple-element.47.refs_3_, f32[128,2]{1,0:T(8,128)S(1)} %copy.17.refs_4_), custom_call_target="tpu_custom_call" | custom-call | flops 335544320 | bytes 1048576 | tf_op jit(solution)/shard_map/pallas_call | solution.py:336
  (111 shorter events, 35.2 us)
Async XLA Ops:
  53.6 8.1 %collective-permute-start.14 = (bf16[64,2048]{1,0:T(8,128)(2,1)}, bf16[64,2048]{1,0:T(8,128)(2,1)S(1)}, u32[]{:S(2)}, u32[]{:S(2)}) collective-permute-start(bf16[64,2048]{1,0:T(8,128)(2,1)} %get-tuple-element.33.refs_0_), channel_id=1, source_target_pairs={{0,1},{1,2},{2,3},{3,0},{4,5},{5,6},{6,7},{7,4},{8,9},{9,10},{10,1... | collective-permute-start | bytes 786440 | tf_op jit(solution)/shard_map/ppermute | solution.py:524
  55.1 24.7 %copy-start = (bf16[1,2048,768]{2,1,0:T(8,128)(2,1)S(1)}, bf16[1,2048,768]{2,1,0:T(8,128)(2,1)}, u32[]{:S(2)}) copy-start(bf16[1,2048,768]{2,1,0:T(8,128)(2,1)} %param.23) | copy-start | bytes 9437188
  55.1 10.1 %collective-permute-start.17 = (bf16[64,2048]{1,0:T(8,128)(2,1)}, bf16[64,2048]{1,0:T(8,128)(2,1)}, u32[]{:S(2)}, u32[]{:S(2)}) collective-permute-start(bf16[64,2048]{1,0:T(8,128)(2,1)} %get-tuple-element.34.refs_1_), channel_id=1, source_target_pairs={{0,3},{1,0},{2,1},{3,2},{4,7},{5,4},{6,5},{7,6},{8,11},{9,8},{10,9... | collective-permute-start | bytes 786440 | tf_op jit(solution)/shard_map/ppermute | solution.py:524
  61.7 7.2 %copy-start.12 = (bf16[64,2048]{1,0:T(8,128)(2,1)}, bf16[64,2048]{1,0:T(8,128)(2,1)S(1)}, u32[]{:S(2)}) copy-start(bf16[64,2048]{1,0:T(8,128)(2,1)S(1)} %collective-permute-done.14.refs_2_) | copy-start | bytes 786436
  61.7 10.4 %collective-permute-start.18 = (bf16[64,2048]{1,0:T(8,128)(2,1)S(1)}, bf16[64,2048]{1,0:T(8,128)(2,1)S(1)}, u32[]{:S(2)}, u32[]{:S(2)}) collective-permute-start(bf16[64,2048]{1,0:T(8,128)(2,1)S(1)} %collective-permute-done.14.refs_2_), channel_id=1, source_target_pairs={{0,1},{1,2},{2,3},{3,0},{4,5},{5,6},{6,7},{7,4},{8,9},{9,10},{10,1... | collective-permute-start | bytes 786440 | tf_op jit(solution)/shard_map/ppermute | solution.py:524
  62.0 25.3 %collective-permute-start.15 = (bf16[64,2048]{1,0:T(8,128)(2,1)}, bf16[64,2048]{1,0:T(8,128)(2,1)}, u32[]{:S(2)}, u32[]{:S(2)}) collective-permute-start(bf16[64,2048]{1,0:T(8,128)(2,1)} %get-tuple-element.34.refs_1_), channel_id=1, source_target_pairs={{0,1},{1,2},{2,3},{3,0},{4,5},{5,6},{6,7},{7,4},{8,9},{9,10},{10,1... | collective-permute-start | bytes 786440 | tf_op jit(solution)/shard_map/ppermute | solution.py:524
  63.5 25.9 %collective-permute-start.16 = (bf16[64,2048]{1,0:T(8,128)(2,1)}, bf16[64,2048]{1,0:T(8,128)(2,1)}, u32[]{:S(2)}, u32[]{:S(2)}) collective-permute-start(bf16[64,2048]{1,0:T(8,128)(2,1)} %get-tuple-element.33.refs_0_), channel_id=1, source_target_pairs={{0,3},{1,0},{2,1},{3,2},{4,7},{5,4},{6,5},{7,6},{8,11},{9,8},{10,9... | collective-permute-start | bytes 786440 | tf_op jit(solution)/shard_map/ppermute | solution.py:524
  65.3 13.4 %collective-permute-start.19 = (bf16[64,2048]{1,0:T(8,128)(2,1)}, bf16[64,2048]{1,0:T(8,128)(2,1)}, u32[]{:S(2)}, u32[]{:S(2)}) collective-permute-start(bf16[64,2048]{1,0:T(8,128)(2,1)} %collective-permute-done.17.refs_5_), channel_id=1, source_target_pairs={{0,3},{1,0},{2,1},{3,2},{4,7},{5,4},{6,5},{7,6},{8,11},{9,8},{10,9... | collective-permute-start | bytes 786440 | tf_op jit(solution)/shard_map/ppermute | solution.py:524
  69.0 50.5 %collective-permute-start.24 = (bf16[192,2048]{1,0:T(8,128)(2,1)}, bf16[192,2048]{1,0:T(8,128)(2,1)}, u32[]{:S(2)}, u32[]{:S(2)}) collective-permute-start(bf16[192,2048]{1,0:T(8,128)(2,1)} %shard_map.155.refs_0_), channel_id=1, source_target_pairs={{0,1},{1,2},{2,3},{3,0},{4,5},{5,6},{6,7},{7,4},{8,9},{9,10},{10,1... | collective-permute-start | bytes 2359304 | tf_op jit(solution)/shard_map/ppermute | solution.py:524
  72.1 49.4 %collective-permute-start.25 = (bf16[192,2048]{1,0:T(8,128)(2,1)}, bf16[192,2048]{1,0:T(8,128)(2,1)}, u32[]{:S(2)}, u32[]{:S(2)}) collective-permute-start(bf16[192,2048]{1,0:T(8,128)(2,1)} %shard_map.155.refs_0_), channel_id=1, source_target_pairs={{0,3},{1,0},{2,1},{3,2},{4,7},{5,4},{6,5},{7,6},{8,11},{9,8},{10,9... | collective-permute-start | bytes 2359304 | tf_op jit(solution)/shard_map/ppermute | solution.py:524
  78.6 162.5 %collective-permute-start.10 = (bf16[256,2048]{1,0:T(8,128)(2,1)}, bf16[256,2048]{1,0:T(8,128)(2,1)}, u32[]{:S(2)}, u32[]{:S(2)}) collective-permute-start(bf16[256,2048]{1,0:T(8,128)(2,1)} %refs_4_.2), channel_id=1, source_target_pairs={{0,1},{1,2},{2,3},{3,0},{4,5},{5,6},{6,7},{7,4},{8,9},{9,10},{10,1... | collective-permute-start | bytes 3145736 | tf_op jit(solution)/shard_map/ppermute | solution.py:524
  79.8 1.9 copy-start.1
  81.7 1.9 copy-start.4
  83.6 5.8 %copy-start.2 = (bf16[1,2048,768]{2,1,0:T(8,128)(2,1)S(1)}, bf16[1,2048,768]{2,1,0:T(8,128)(2,1)}, u32[]{:S(2)}) copy-start(bf16[1,2048,768]{2,1,0:T(8,128)(2,1)} %param.24) | copy-start | bytes 9437188
  83.6 5.8 %copy-start.13 = (bf16[64,2048]{1,0:T(8,128)(2,1)S(1)}, bf16[64,2048]{1,0:T(8,128)(2,1)}, u32[]{:S(2)}) copy-start(bf16[64,2048]{1,0:T(8,128)(2,1)} %copy-done.12) | copy-start | bytes 786436
  87.3 10.7 %collective-permute-start.22 = (bf16[64,2048]{1,0:T(8,128)(2,1)S(1)}, bf16[64,2048]{1,0:T(8,128)(2,1)S(1)}, u32[]{:S(2)}, u32[]{:S(2)}) collective-permute-start(bf16[64,2048]{1,0:T(8,128)(2,1)S(1)} %get-tuple-element.39), channel_id=1, source_target_pairs={{0,3},{1,0},{2,1},{3,2},{4,7},{5,4},{6,5},{7,6},{8,11},{9,8},{10,9... | collective-permute-start | bytes 786440 | tf_op jit(solution)/shard_map/ppermute | solution.py:524
  89.4 29.9 %collective-permute-start.20 = (bf16[64,2048]{1,0:T(8,128)(2,1)S(1)}, bf16[64,2048]{1,0:T(8,128)(2,1)S(1)}, u32[]{:S(2)}, u32[]{:S(2)}) collective-permute-start(bf16[64,2048]{1,0:T(8,128)(2,1)S(1)} %get-tuple-element.37), channel_id=1, source_target_pairs={{0,1},{1,2},{2,3},{3,0},{4,5},{5,6},{6,7},{7,4},{8,9},{9,10},{10,1... | collective-permute-start | bytes 786440 | tf_op jit(solution)/shard_map/ppermute | solution.py:524
  98.1 49.2 %collective-permute-start.23 = (bf16[128,2048]{1,0:T(8,128)(2,1)S(1)}, bf16[128,2048]{1,0:T(8,128)(2,1)S(1)}, u32[]{:S(2)}, u32[]{:S(2)}) collective-permute-start(bf16[128,2048]{1,0:T(8,128)(2,1)S(1)} %shard_map.153), channel_id=1, source_target_pairs={{0,3},{1,0},{2,1},{3,2},{4,7},{5,4},{6,5},{7,6},{8,11},{9,8},{10,9... | collective-permute-start | bytes 1572872 | tf_op jit(solution)/shard_map/ppermute | solution.py:524
  119.4 27.9 %collective-permute-start.21 = (bf16[128,2048]{1,0:T(8,128)(2,1)S(1)}, bf16[128,2048]{1,0:T(8,128)(2,1)S(1)}, u32[]{:S(2)}, u32[]{:S(2)}) collective-permute-start(bf16[128,2048]{1,0:T(8,128)(2,1)S(1)} %shard_map.152), channel_id=1, source_target_pairs={{0,1},{1,2},{2,3},{3,0},{4,5},{5,6},{6,7},{7,4},{8,9},{9,10},{10,1... | collective-permute-start | bytes 1572872 | tf_op jit(solution)/shard_map/ppermute | solution.py:524
  120.6 19.3 %collective-permute-start.26 = (bf16[96,2048]{1,0:T(8,128)(2,1)S(1)}, bf16[96,2048]{1,0:T(8,128)(2,1)S(1)}, u32[]{:S(2)}, u32[]{:S(2)}) collective-permute-start(bf16[96,2048]{1,0:T(8,128)(2,1)S(1)} %slice.38), channel_id=1, source_target_pairs={{0,1},{1,2},{2,3},{3,0},{4,5},{5,6},{6,7},{7,4},{8,9},{9,10},{10,1... | collective-permute-start | bytes 1179656 | tf_op jit(solution)/shard_map/ppermute | solution.py:524
  122.6 17.3 %collective-permute-start.27 = (bf16[96,2048]{1,0:T(8,128)(2,1)S(1)}, bf16[96,2048]{1,0:T(8,128)(2,1)S(1)}, u32[]{:S(2)}, u32[]{:S(2)}) collective-permute-start(bf16[96,2048]{1,0:T(8,128)(2,1)S(1)} %slice.39), channel_id=1, source_target_pairs={{0,3},{1,0},{2,1},{3,2},{4,7},{5,4},{6,5},{7,6},{8,11},{9,8},{10,9... | collective-permute-start | bytes 1179656 | tf_op jit(solution)/shard_map/ppermute | solution.py:524
  144.1 33.7 %collective-permute-start.28 = (bf16[96,2048]{1,0:T(8,128)(2,1)}, bf16[96,2048]{1,0:T(8,128)(2,1)}, u32[]{:S(2)}, u32[]{:S(2)}) collective-permute-start(bf16[96,2048]{1,0:T(8,128)(2,1)} %get-tuple-element.42), channel_id=1, source_target_pairs={{0,1},{1,2},{2,3},{3,0},{4,5},{5,6},{6,7},{7,4},{8,9},{9,10},{10,1... | collective-permute-start | bytes 1179656 | tf_op jit(solution)/shard_map/ppermute | solution.py:524
  144.1 35.0 %collective-permute-start.32 = (bf16[96,2048]{1,0:T(8,128)(2,1)}, bf16[96,2048]{1,0:T(8,128)(2,1)}, u32[]{:S(2)}, u32[]{:S(2)}) collective-permute-start(bf16[96,2048]{1,0:T(8,128)(2,1)} %get-tuple-element.46), channel_id=1, source_target_pairs={{0,3},{1,0},{2,1},{3,2},{4,7},{5,4},{6,5},{7,6},{8,11},{9,8},{10,9... | collective-permute-start | bytes 1179656 | tf_op jit(solution)/shard_map/ppermute | solution.py:524
  149.3 48.3 %all-to-all-start.1 = ((bf16[64,32,128]{2,1,0:T(8,128)(2,1)}), bf16[64,32,128]{2,1,0:T(8,128)(2,1)}, u32[]{:S(2)}, u32[]{:S(2)}) async-start(bf16[64,32,128]{2,1,0:T(8,128)(2,1)} %bitcast.31), calls=%async_computation.1 | async-start | bytes 1048576 | tf_op jit(solution)/shard_map/all_to_all | solution.py:599
  160.0 1.9 copy-start.3
  174.4 13.3 %collective-permute-start.30 = (bf16[96,2048]{1,0:T(8,128)(2,1)S(1)}, bf16[96,2048]{1,0:T(8,128)(2,1)S(1)}, u32[]{:S(2)}, u32[]{:S(2)}) collective-permute-start(bf16[96,2048]{1,0:T(8,128)(2,1)S(1)} %get-tuple-element.43), channel_id=1, source_target_pairs={{0,1},{1,2},{2,3},{3,0},{4,5},{5,6},{6,7},{7,4},{8,9},{9,10},{10,1... | collective-permute-start | bytes 1179656 | tf_op jit(solution)/shard_map/ppermute | solution.py:524
  174.5 13.2 %collective-permute-start.31 = (bf16[96,2048]{1,0:T(8,128)(2,1)S(1)}, bf16[96,2048]{1,0:T(8,128)(2,1)S(1)}, u32[]{:S(2)}, u32[]{:S(2)}) collective-permute-start(bf16[96,2048]{1,0:T(8,128)(2,1)S(1)} %get-tuple-element.44), channel_id=1, source_target_pairs={{0,3},{1,0},{2,1},{3,2},{4,7},{5,4},{6,5},{7,6},{8,11},{9,8},{10,9... | collective-permute-start | bytes 1179656 | tf_op jit(solution)/shard_map/ppermute | solution.py:524
  177.7 10.0 %copy-start.7 = (bf16[256,2048]{1,0:T(8,128)(2,1)S(1)}, bf16[256,2048]{1,0:T(8,128)(2,1)}, u32[]{:S(2)}) copy-start(bf16[256,2048]{1,0:T(8,128)(2,1)} %refs_4_.2) | copy-start | bytes 3145732
  178.9 16.3 %collective-permute-start.29 = (bf16[96,2048]{1,0:T(8,128)(2,1)S(1)}, bf16[96,2048]{1,0:T(8,128)(2,1)S(1)}, u32[]{:S(2)}, u32[]{:S(2)}) collective-permute-start(bf16[96,2048]{1,0:T(8,128)(2,1)S(1)} %shard_map.158), channel_id=1, source_target_pairs={{0,1},{1,2},{2,3},{3,0},{4,5},{5,6},{6,7},{7,4},{8,9},{9,10},{10,1... | collective-permute-start | bytes 1179656 | tf_op jit(solution)/shard_map/ppermute | solution.py:524
  180.1 15.5 %collective-permute-start.33 = (bf16[96,2048]{1,0:T(8,128)(2,1)S(1)}, bf16[96,2048]{1,0:T(8,128)(2,1)S(1)}, u32[]{:S(2)}, u32[]{:S(2)}) collective-permute-start(bf16[96,2048]{1,0:T(8,128)(2,1)S(1)} %shard_map.159), channel_id=1, source_target_pairs={{0,3},{1,0},{2,1},{3,2},{4,7},{5,4},{6,5},{7,6},{8,11},{9,8},{10,9... | collective-permute-start | bytes 1179656 | tf_op jit(solution)/shard_map/ppermute | solution.py:524
  187.7 55.3 %collective-permute-start.11 = (bf16[256,2048]{1,0:T(8,128)(2,1)S(1)}, bf16[256,2048]{1,0:T(8,128)(2,1)S(1)}, u32[]{:S(2)}, u32[]{:S(2)}) collective-permute-start(bf16[256,2048]{1,0:T(8,128)(2,1)S(1)} %copy-done.7), channel_id=1, source_target_pairs={{0,3},{1,0},{2,1},{3,2},{4,7},{5,4},{6,5},{7,6},{8,11},{9,8},{10,9... | collective-permute-start | bytes 3145736 | tf_op jit(solution)/shard_map/ppermute | solution.py:524
  195.7 12.2 %copy-start.10 = (bf16[1024,128]{1,0:T(8,128)(2,1)S(1)}, bf16[1024,128]{1,0:T(8,128)(2,1)}, u32[]{:S(2)}) copy-start(bf16[1024,128]{1,0:T(8,128)(2,1)} %q_ref.1) | copy-start | bytes 786436
  195.7 12.2 %copy-start.16 = (f32[2]{0:T(128)S(1)}, f32[2]{0:T(128)}, u32[]{:S(2)}) copy-start(f32[2]{0:T(128)} %r_ref.2) | copy-start | bytes 28
  197.6 97.0 %all-to-all-start.2 = ((bf16[64,48,128]{2,1,0:T(8,128)(2,1)}), bf16[64,48,128]{2,1,0:T(8,128)(2,1)S(1)}, u32[]{:S(2)}, u32[]{:S(2)}) async-start(bf16[64,48,128]{2,1,0:T(8,128)(2,1)} %bitcast.13), calls=%async_computation.2 | async-start | bytes 1572864 | tf_op jit(solution)/shard_map/all_to_all | solution.py:599
  209.9 64.5 %copy-start.15 = (f32[256]{0:T(256)S(1)}, f32[256]{0:T(256)}, u32[]{:S(2)}) copy-start(f32[256]{0:T(256)} %param.17) | copy-start | bytes 3076
  220.7 1.3 collective-permute-start
  222.5 6.4 %collective-permute-start.1 = (f32[128,128]{1,0:T(8,128)S(1)}, f32[128,128]{1,0:T(8,128)S(1)}, u32[]{:S(2)}, u32[]{:S(2)}) collective-permute-start(f32[128,128]{1,0:T(8,128)S(1)} %shard_map.141), channel_id=1, source_target_pairs={{0,8},{8,16},{16,24},{24,32},{32,40},{40,48},{48,56},{56,64},{64,7... | collective-permute-start | bytes 196616 | tf_op jit(solution)/shard_map/ppermute | solution.py:613
  228.9 6.1 %collective-permute-start.2 = (f32[128,128]{1,0:T(8,128)S(1)}, f32[128,128]{1,0:T(8,128)S(1)}, u32[]{:S(2)}, u32[]{:S(2)}) collective-permute-start(f32[128,128]{1,0:T(8,128)S(1)} %collective-permute-done.1.f_ref), channel_id=1, source_target_pairs={{0,8},{8,16},{16,24},{24,32},{32,40},{40,48},{48,56},{56,64},{64,7... | collective-permute-start | bytes 196616 | tf_op jit(solution)/shard_map/ppermute | solution.py:613
  235.6 12.0 %collective-permute-start.3 = (f32[128,128]{1,0:T(8,128)S(1)}, f32[128,128]{1,0:T(8,128)S(1)}, u32[]{:S(2)}, u32[]{:S(2)}) collective-permute-start(f32[128,128]{1,0:T(8,128)S(1)} %shard_map.142.f_ref), channel_id=1, source_target_pairs={{0,16},{8,24},{16,32},{24,40},{32,48},{40,56},{48,64},{56,72},{64,... | collective-permute-start | bytes 196616 | tf_op jit(solution)/shard_map/ppermute | solution.py:613
  243.0 46.0 %collective-permute-start.12 = (bf16[128,2048]{1,0:T(8,128)(2,1)}, bf16[128,2048]{1,0:T(8,128)(2,1)}, u32[]{:S(2)}, u32[]{:S(2)}) collective-permute-start(bf16[128,2048]{1,0:T(8,128)(2,1)} %slice.36), channel_id=1, source_target_pairs={{0,1},{1,2},{2,3},{3,0},{4,5},{5,6},{6,7},{7,4},{8,9},{9,10},{10,1... | collective-permute-start | bytes 1572872 | tf_op jit(solution)/shard_map/ppermute | solution.py:524
  243.9 45.1 %collective-permute-start.13 = (bf16[128,2048]{1,0:T(8,128)(2,1)}, bf16[128,2048]{1,0:T(8,128)(2,1)}, u32[]{:S(2)}, u32[]{:S(2)}) collective-permute-start(bf16[128,2048]{1,0:T(8,128)(2,1)} %slice.37), channel_id=1, source_target_pairs={{0,3},{1,0},{2,1},{3,2},{4,7},{5,4},{6,5},{7,6},{8,11},{9,8},{10,9... | collective-permute-start | bytes 1572872 | tf_op jit(solution)/shard_map/ppermute | solution.py:524
  248.2 5.1 %collective-permute-start.4 = (f32[128,128]{1,0:T(8,128)S(1)}, f32[128,128]{1,0:T(8,128)S(1)}, u32[]{:S(2)}, u32[]{:S(2)}) collective-permute-start(f32[128,128]{1,0:T(8,128)S(1)} %shard_map.143.f_ref), channel_id=1, source_target_pairs={{0,32},{8,40},{16,48},{24,56},{32,64},{40,72},{48,80},{56,88},{64,... | collective-permute-start | bytes 196616 | tf_op jit(solution)/shard_map/ppermute | solution.py:613
  253.8 8.3 %collective-permute-start.5 = (f32[128,128]{1,0:T(8,128)S(1)}, f32[128,128]{1,0:T(8,128)S(1)}, u32[]{:S(2)}, u32[]{:S(2)}) collective-permute-start(f32[128,128]{1,0:T(8,128)S(1)} %shard_map.144.f_ref), channel_id=1, source_target_pairs={{0,64},{8,72},{16,80},{24,88},{32,96},{40,104},{48,112},{56,120},{... | collective-permute-start | bytes 196616 | tf_op jit(solution)/shard_map/ppermute | solution.py:613
  262.7 11.7 %collective-permute-start.6 = (f32[128,128]{1,0:T(8,128)S(1)}, f32[128,128]{1,0:T(8,128)S(1)}, u32[]{:S(2)}, u32[]{:S(2)}) collective-permute-start(f32[128,128]{1,0:T(8,128)S(1)} %shard_map.145.f_ref), channel_id=1, source_target_pairs={{0,128},{8,136},{16,144},{24,152},{32,160},{40,168},{48,176},{56,1... | collective-permute-start | bytes 196616 | tf_op jit(solution)/shard_map/ppermute | solution.py:613
  276.6 7.0 %copy-start.23 = (f32[128,2]{0,1:T(2,128)S(1)}, f32[128,2]{0,1:T(2,128)}, u32[]{:S(2)}) copy-start(f32[128,2]{0,1:T(2,128)} %param.22) | copy-start | bytes 3076
  279.2 6.4 %collective-permute-start.7 = (bf16[256,256]{1,0:T(8,128)(2,1)}, bf16[256,256]{1,0:T(8,128)(2,1)S(1)}, u32[]{:S(2)}, u32[]{:S(2)}) collective-permute-start(bf16[256,256]{1,0:T(8,128)(2,1)} %get-tuple-element.29), channel_id=1, source_target_pairs={{0,1},{1,2},{2,3},{3,0},{4,5},{5,6},{6,7},{7,4},{8,9},{9,10},{10,1... | collective-permute-start | bytes 393224 | tf_op jit(solution)/shard_map/ppermute | solution.py:524
  279.2 6.4 %collective-permute-start.8 = (bf16[256,256]{1,0:T(8,128)(2,1)}, bf16[256,256]{1,0:T(8,128)(2,1)S(1)}, u32[]{:S(2)}, u32[]{:S(2)}) collective-permute-start(bf16[256,256]{1,0:T(8,128)(2,1)} %get-tuple-element.30), channel_id=1, source_target_pairs={{0,3},{1,0},{2,1},{3,2},{4,7},{5,4},{6,5},{7,6},{8,11},{9,8},{10,9... | collective-permute-start | bytes 393224 | tf_op jit(solution)/shard_map/ppermute | solution.py:524
  282.5 6.6 %collective-permute-start.9 = (bf16[256,256]{1,0:T(8,128)(2,1)S(1)}, bf16[256,256]{1,0:T(8,128)(2,1)}, u32[]{:S(2)}, u32[]{:S(2)}) collective-permute-start(bf16[256,256]{1,0:T(8,128)(2,1)S(1)} %get-tuple-element.31), channel_id=1, source_target_pairs={{0,2},{1,3},{2,0},{3,1},{4,6},{5,7},{6,4},{7,5},{8,10},{9,11},{10,... | collective-permute-start | bytes 393224 | tf_op jit(solution)/shard_map/ppermute | solution.py:524
  (12 other events, 12.0 us)
